TPU v7x, 256 devices: a whole 4x4x8 slice. The times are simulated.
256 devices in a mesh: kv: 64 (over z, x, core), tp: 4 (over y).
Axes of the slice: x: 4, y: 4, z: 8, core: 2. Of those that a mesh axis runs over, the one named last changes fastest.
Arguments:
- hidden: bfloat16 [1024, 4, 2048], P(None, None, 'kv'), may hold values from -18 to 18
- norm_gain: float32 [2048], replicated, may hold values from 0.1 to 1.9
- w_query: bfloat16 [2048, 1024], P(None, 'tp'), may hold values from -0.125 to 0.125
- w_forget: bfloat16 [2048, 1024], P(None, 'tp'), may hold values from -0.125 to 0.125
- w_input: bfloat16 [2048, 1024], P(None, 'tp'), may hold values from -0.125 to 0.125
- w_outgate: bfloat16 [2048, 1024], P(None, 'tp'), may hold values from -0.125 to 0.125
- w_out: bfloat16 [1024, 2048], replicated, may hold values from -0.1875 to 0.1875
- floor: float32 [1024], P('tp'), may hold values from 0 to 0.95
- head_gain: float32 [128], replicated, may hold values from 0.1 to 1.9
- base_state: float32 [1024, 8, 128, 128], P('kv', 'tp'), may hold values from -4 to 4
- prev_forget: bfloat16 [1024, 4, 1024], P('kv', None, 'tp'), may hold values from -6 to 6
- prev_input: bfloat16 [1024, 4, 1024], P('kv', None, 'tp'), may hold values from -6 to 6
- accepted: int32 [1024], P('kv'), may hold values from 0 to 4
Outputs:
- mixed: bfloat16 [1024, 4, 2048], P(None, None, 'kv')
- taken_state: float32 [1024, 8, 128, 128], P('kv', 'tp')
All inputs are finite; a program needn't handle non-finite values.
Results may differ from a plain program's by a relative error of at most 0.014.
Values may be sent and summed in bfloat16 or wider, within the bound.
A program may use at most 64 MiB of HBM per device.

v0:
```python
import jax
import jax.numpy as jnp
from jax import lax
from jax.sharding import Mesh
from jax.sharding import PartitionSpec as P

D = 2048
HEAD_DIM = 128
PROPS = 4
KV = ("kv_0", "kv_1", "kv_2")


def copy_for_each(array, axis):
    copies = jnp.broadcast_to(array, (lax.axis_size(axis), *array.shape))
    return lax.all_to_all(copies, axis, split_axis=0, concat_axis=0, tiled=True)


def in_order(pieces, dim):
    shape = list(pieces.shape[1:])
    shape[dim] *= pieces.shape[0]
    return jnp.moveaxis(pieces, 0, dim).reshape(shape)


def collect(array, axis, dim):
    pieces = copy_for_each(array, axis)
    return in_order(pieces, dim)


def split_up(array, dim, length):
    shape = array.shape
    pieces = array.reshape(*shape[:dim], length, shape[dim] // length, *shape[dim + 1 :])
    return jnp.moveaxis(pieces, dim, 0)


def turned_blocks(pieces, axes, turns):
    inside = pieces.shape[1:]
    whole = pieces.reshape(*(lax.axis_size(a) for a in axes), *inside)
    for k in turns:
        whole = lax.all_to_all(whole, axes[k], k, k, tiled=True)
    return whole.reshape(-1, *inside)


def two_step_exchange(array, groups, turns, split_dim, concat_dim):
    length = lax.axis_size(groups[0]) * lax.axis_size(groups[1])
    pieces = split_up(array, split_dim, length)
    return in_order(turned_blocks(pieces, groups, turns), concat_dim)


def shards(
    hidden,
    norm_gain,
    w_query,
    w_forget,
    w_input,
    w_outgate,
    w_out,
    floor,
    head_gain,
    base_state,
    prev_forget,
    prev_input,
    accepted,
):
    kv_count = lax.axis_size(KV)
    tp_count = lax.axis_size("tp")
    tp_place = lax.axis_index("tp")
    columns = hidden.shape[2]
    grouped = hidden.reshape(kv_count, tp_count, -1, PROPS, columns)
    source = lax.dynamic_index_in_dim(grouped, tp_place, 1, keepdims=False).reshape(
        -1, PROPS, columns
    )
    own_part = lax.all_to_all(source, KV, split_axis=0, concat_axis=2, tiled=True)
    arrived = collect(own_part, "tp", 0)
    whole_vals = arrived.astype(jnp.float32)
    row_sums = jnp.sum(whole_vals * whole_vals, axis=2)
    normed = (whole_vals * lax.rsqrt(row_sums / D + 1e-06)[..., None] * norm_gain).astype(
        jnp.bfloat16
    )
    query_pre = jnp.dot(normed, w_query, preferred_element_type=jnp.float32).astype(jnp.bfloat16)
    forget_pre = jnp.dot(normed, w_forget, preferred_element_type=jnp.float32).astype(jnp.bfloat16)
    input_pre = jnp.dot(normed, w_input, preferred_element_type=jnp.float32).astype(jnp.bfloat16)
    gate_pre = jnp.dot(normed, w_outgate, preferred_element_type=jnp.float32).astype(jnp.bfloat16)
    seq_local = normed.shape[0]
    head_local = w_query.shape[1] // HEAD_DIM
    shape = (seq_local, PROPS, head_local, HEAD_DIM)
    query = jax.nn.silu(query_pre.astype(jnp.float32)).reshape(shape)
    forget = (floor + (1.0 - floor) * jax.nn.sigmoid(forget_pre.astype(jnp.float32))).reshape(shape)
    value = input_pre.astype(jnp.float32).reshape(shape)
    prev_f = (floor + (1.0 - floor) * jax.nn.sigmoid(prev_forget.astype(jnp.float32))).reshape(
        shape
    )
    prev_v = prev_input.astype(jnp.float32).reshape(shape)
    state = base_state
    for step in range(PROPS):
        live = (step < accepted)[:, None, None, None]
        moved = (
            prev_f[:, step][..., None] * state
            + (1.0 - prev_f[:, step])[..., None] * prev_v[:, step][:, :, None, :]
        )
        state = jnp.where(live, moved, state)
    taken_state = state
    outputs = []
    for step in range(PROPS):
        state = (
            forget[:, step][..., None] * state
            + (1.0 - forget[:, step])[..., None] * value[:, step][:, :, None, :]
        )
        outputs.append(
            jnp.einsum("bhk,bhkv->bhv", query[:, step], state, precision=lax.Precision.HIGHEST)
        )
    result = jnp.stack(outputs, axis=1)
    scaled = (
        result * lax.rsqrt(jnp.mean(result * result, axis=-1, keepdims=True) + 1e-05) * head_gain
    )
    gated = scaled * jax.nn.silu(gate_pre.astype(jnp.float32)).reshape(shape)
    mixed_heads = gated.reshape(seq_local, PROPS, head_local * HEAD_DIM).astype(jnp.bfloat16)
    regrouped = lax.all_to_all(mixed_heads, "tp", split_axis=0, concat_axis=2, tiled=True)
    piece = jnp.dot(regrouped, w_out, preferred_element_type=jnp.float32).astype(jnp.bfloat16)
    spread_out = two_step_exchange(piece, (("kv_0", "kv_1"), "kv_2"), (1, 0), 2, 0)
    width_part = spread_out.shape[2]
    stacked = spread_out.reshape(kv_count, 1, -1, PROPS, width_part)
    collected = lax.all_gather(stacked, "tp", axis=1, tiled=True)
    mixed = collected.reshape(-1, PROPS, width_part)
    return (mixed, taken_state)


def solution(mesh):
    torus = Mesh(mesh.devices.reshape(8, 4, 2, mesh.shape["tp"]), ("kv_0", "kv_1", "kv_2", "tp"))
    in_specs = (
        P(None, None, KV),
        P(),
        P(None, "tp"),
        P(None, "tp"),
        P(None, "tp"),
        P(None, "tp"),
        P(),
        P("tp"),
        P(),
        P(KV, "tp", None, None),
        P(KV, None, "tp"),
        P(KV, None, "tp"),
        P(KV),
    )
    out_specs = (P(None, None, KV), P(KV, "tp", None, None))
    return jax.shard_map(
        shards, mesh=torus, in_specs=in_specs, out_specs=out_specs, check_vma=False
    )
```

profile of v0, /device:TPU:32, one launch (start us, length us, event | category | flops | bytes accessed | tf_op | source)
XLA Modules:
  0.0 115.3 jit_solution(15012562396908254183)
XLA Ops:
  0.7 1.5 %copy.100 = bf16[1024,4,32]{2,0,1:T(8,128)(2,1)S(1)} copy(bf16[1024,4,32]{0,2,1:T(8,128)(2,1)} %param.13) | data formatting | bytes 524288 | tf_op args[0]
  2.5 0.8 reshape.174
  3.3 11.6 %all-to-all-start = ((bf16[64,2,256]{2,1,0:T(2,128)(2,1)}), bf16[64,2,256]{2,1,0:T(2,128)(2,1)S(1)}, u32[]{:S(2)}, u32[]{:S(2)}) async-start(bf16[64,2,256]{2,1,0:T(2,128)(2,1)} %reshape.174), calls=%async_computation | async-start | bytes 131072 | tf_op jit(solution)/shard_map/all_to_all | solution.py:72
  15.2 7.0 %add_select_fusion = f32[16,2,128,128]{3,2,1,0:T(8,128)S(1)} fusion(f32[16,2,128,128]{3,2,1,0:T(8,128)} %param.22, f32[16,2,128]{2,1,0:T(2,128)S(1)} %get-tuple-element.39, f32[16,2,128]{2,1,0:T(2,128)S(1)} %get-tuple-element.35, f32[16,2,128]{2,1,0:T(2,128)S(1)} %get-tuple-element.37, f32[16,2,128]{2,1,0:T(2,128)S(1)} %get-tuple-element.34, ...), kind=kLoop, calls=%fused_computation.10 | loop fusion | flops 8388608 | bytes 4390976 | tf_op jit(solution)/shard_map/jit(_where)/select_n | solution.py:100
  22.3 1.8 %all-to-all-done = bf16[64,2,256]{2,1,0:T(2,128)(2,1)S(1)} async-done(((bf16[64,2,256]{2,1,0:T(2,128)(2,1)}), bf16[64,2,256]{2,1,0:T(2,128)(2,1)S(1)}, u32[]{:S(2)}, u32[]{:S(2)}) %all-to-all-start) | async-done | bytes 65568 | tf_op jit(solution)/shard_map/all_to_all | solution.py:72
  24.4 0.3 reshape.172
  24.6 0.8 broadcast_in_dim.25
  25.4 4.5 %all-to-all-start.1 = ((bf16[4,4,4,2048]{3,1,2,0:T(4,128)(2,1)}), bf16[4,4,4,2048]{3,1,2,0:T(4,128)(2,1)S(1)}, u32[]{:S(2)}, u32[]{:S(2)}) async-start(bf16[4,4,4,2048]{3,1,2,0:T(4,128)(2,1)} %broadcast_in_dim.25), calls=%async_computation.1 | async-start | bytes 524288 | tf_op jit(solution)/shard_map/all_to_all | solution.py:15
  29.9 6.9 %all-to-all-done.1 = bf16[4,4,4,2048]{3,1,2,0:T(4,128)(2,1)S(1)} async-done(((bf16[4,4,4,2048]{3,1,2,0:T(4,128)(2,1)}), bf16[4,4,4,2048]{3,1,2,0:T(4,128)(2,1)S(1)}, u32[]{:S(2)}, u32[]{:S(2)}) %all-to-all-start.1) | async-done | bytes 262176 | tf_op jit(solution)/shard_map/all_to_all | solution.py:15
  36.9 0.2 multiply_reduce_fusion
  37.4 0.3 fusion.38
  37.7 0.3 fusion.19
  38.1 1.5 %fusion.12 = f32[16,4,256]{2,0,1:T(8,128)S(1)} fusion(bf16[16,4,2048]{2,0,1:T(8,128)(2,1)S(1)} %fusion.38, bf16[2048,256]{1,0:T(8,128)(2,1)} %param.17), kind=kOutput, calls=%fused_computation.16 | convolution fusion | flops 67141632 | bytes 1376256 | tf_op jit(solution)/shard_map/dot_general | solution.py:81
  39.6 0.7 reshape.158
  40.3 2.2 %divide_multiply_fusion = f32[16,4,256]{2,0,1:T(8,128)} fusion(bf16[16,4,2048]{2,0,1:T(8,128)(2,1)S(1)} %fusion.38, bf16[2048,256]{1,0:T(8,128)(2,1)} %param.15), kind=kOutput, calls=%fused_computation.55 | convolution fusion | flops 67207168 | bytes 1376256 | tf_op jit(solution)/shard_map/dot_general | solution.py:79
  42.5 0.9 reshape.144
  43.4 0.8 slice_bitcast_fusion.6
  44.2 2.8 %fusion.9 = f32[16,2,1,128]{3,2,1,0:T(1,128)S(1)} fusion(f32[16,2,128,1]{2,3,1,0:T(1,128)S(1)} %bitcast.170, f32[16,2,128,128]{3,2,1,0:T(8,128)S(1)} %add_select_fusion, f32[16,2,128]{2,1,0:T(2,128)S(1)} %get-tuple-element.24, f32[16,2,128]{2,1,0:T(2,128)S(1)} %get-tuple-element.20, f32[16,2,128]{2,1,0:T(2,128)S(1)} %get-tuple-element.47), kind=kOutput, calls=%fused_computation.11 | convolution fusion | flops 7864320 | bytes 2179072 | tf_op jit(solution)/shard_map/bhk,bhkv->bhv/dot_general | solution.py:109
  47.0 4.3 %fusion.39 = f32[16,2,1,128]{3,2,1,0:T(1,128)S(1)} fusion(f32[16,2,128,1]{2,3,1,0:T(1,128)S(1)} %bitcast.179, f32[16,2,128,128]{3,2,1,0:T(8,128)S(1)} %add_select_fusion, f32[16,2,128]{2,1,0:T(2,128)S(1)} %get-tuple-element.27, f32[16,2,128]{2,1,0:T(2,128)S(1)} %get-tuple-element.23, f32[16,2,128]{2,1,0:T(2,128)S(1)} %get-tuple-element.44, ...), kind=kOutput, calls=%fused_computation.47 | convolution fusion | flops 9437184 | bytes 2228224 | tf_op jit(solution)/shard_map/bhk,bhkv->bhv/dot_general | solution.py:109
  51.2 6.1 %fusion.10 = f32[16,2,1,128]{3,2,1,0:T(1,128)S(1)} fusion(f32[16,2,128,1]{2,3,1,0:T(1,128)S(1)} %bitcast.178, f32[16,2,128]{2,1,0:T(2,128)S(1)} %get-tuple-element.26, f32[16,2,128]{2,1,0:T(2,128)S(1)} %get-tuple-element.22, f32[16,2,128]{2,1,0:T(2,128)S(1)} %get-tuple-element.45, f32[16,2,128,128]{3,2,1,0:T(8,128)S(1)} %add_select_fusion, ...), kind=kOutput, calls=%fused_computation.12 | convolution fusion | flops 11010048 | bytes 2277376 | tf_op jit(solution)/shard_map/bhk,bhkv->bhv/dot_general | solution.py:109
  57.3 7.2 %fusion.5 = f32[16,2,1,128]{3,2,1,0:T(1,128)S(1)} fusion(f32[16,2,128,1]{2,3,1,0:T(1,128)S(1)} %bitcast.177, f32[16,2,128]{2,1,0:T(2,128)S(1)} %get-tuple-element.25, f32[16,2,128]{2,1,0:T(2,128)S(1)} %get-tuple-element.21, f32[16,2,128]{2,1,0:T(2,128)S(1)} %get-tuple-element.46, f32[16,2,128]{2,1,0:T(2,128)S(1)} %get-tuple-element.26, ...), kind=kOutput, calls=%fused_computation.3 | convolution fusion | flops 12582912 | bytes 2326528 | tf_op jit(solution)/shard_map/bhk,bhkv->bhv/dot_general | solution.py:109
  65.0 1.5 %fusion.42 = bf16[16,4,256]{2,0,1:T(8,128)(2,1)S(1)} fusion(f32[16,4,256]{2,0,1:T(8,128)S(1)} %mul.339, f32[16,1,256]{2,0,1:T(8,128)S(1)} %stack.28, f32[16,1,256]{2,0,1:T(8,128)S(1)} %stack.27, f32[16,1,256]{2,0,1:T(8,128)S(1)} %stack.26, f32[16,1,256]{2,0,1:T(8,128)S(1)} %stack.25, bf16[16,4,2048]{2,0,1:T(8,128)(2,1)S(1)} %fusion.38, ...), kind=kOutput, calls=%fused_computation.51 | convolution fusion | flops 67321856 | bytes 1475584 | tf_op jit(solution)/shard_map/dot_general | solution.py:82
  66.6 7.8 %all_to_all.51 = bf16[16,4,256]{2,1,0:T(4,128)(2,1)S(1)} all-to-all(bf16[16,4,256]{2,1,0:T(4,128)(2,1)S(1)} %copy.113), channel_id=1, replica_groups=mesh['kv_0'=8,'kv_1'=4,'kv_2'=2,'tp'=4] {'tp'}, dimensions={0} | all-to-all | bytes 65536 | tf_op jit(solution)/shard_map/all_to_all | solution.py:117
  74.4 2.9 %fusion.2 = bf16[4,4,2048]{2,1,0:T(4,128)(2,1)S(1)} fusion(bf16[4,4,1024]{2,1,0:T(4,128)(2,1)S(1)} %all_to_all.43, bf16[1024,2048]{1,0:T(8,128)(2,1)} %param.19), kind=kOutput, calls=%fused_computation.2 | convolution fusion | flops 67141632 | bytes 4292608 | tf_op jit(solution)/shard_map/dot_general | solution.py:118
  77.6 0.3 reshape.176
  77.9 3.8 %all_to_all.52 = bf16[2,2,8192]{2,1,0:T(2,128)(2,1)S(1)} all-to-all(bf16[2,2,8192]{2,1,0:T(2,128)(2,1)S(1)} %reshape.176), channel_id=1, replica_groups=mesh['kv_0'=8,'kv_1'=4,'kv_2'=2,'tp'=4] {'kv_2'}, dimensions={0} | all-to-all | bytes 131072 | tf_op jit(solution)/shard_map/all_to_all | solution.py:39
  81.8 0.3 copy.145
  82.3 17.0 %all_to_all.53 = bf16[32,2,512]{2,1,0:T(2,128)(2,1)S(1)} all-to-all(bf16[32,2,512]{2,1,0:T(2,128)(2,1)S(1)} %reshape.178), channel_id=1, replica_groups=mesh['kv_0'=8,'kv_1'=4,'kv_2'=2,'tp'=4] {'kv_0','kv_1'}, dimensions={0} | all-to-all | bytes 131072 | tf_op jit(solution)/shard_map/all_to_all | solution.py:39
  99.5 0.2 copy.117
  99.9 13.4 %all_gather.3 = bf16[64,4,4,4,32]{0,4,3,2,1:T(8,128)(2,1)S(1)} all-gather(bf16[64,1,4,4,32]{0,4,3,2,1:T(8,128)(2,1)S(1)} %copy.118), channel_id=1, replica_groups=mesh['kv_0'=8,'kv_1'=4,'kv_2'=2,'tp'=4] {'tp'}, dimensions={1}, use_global_device_ids=true | all-gather | bytes 327680 | tf_op jit(solution)/shard_map/all_gather | solution.py:122
  113.3 0.9 copy.119
  114.3 1.0 copy.120
  (54 shorter events, 2.6 us)
Async XLA Ops:
  0.6 37.1 %copy-start = (bf16[2048,256]{1,0:T(8,128)(2,1)S(1)}, bf16[2048,256]{1,0:T(8,128)(2,1)}, u32[]{:S(2)}) copy-start(bf16[2048,256]{1,0:T(8,128)(2,1)} %param.16) | copy-start | bytes 3145732
  0.6 14.3 %copy-start.4 = (f32[256]{0:T(256)S(1)}, f32[256]{0:T(256)}, u32[]{:S(2)}) copy-start(f32[256]{0:T(256)} %param.20) | copy-start | bytes 3076
  0.7 14.3 %copy-start.2 = (bf16[16,4,256]{2,1,0:T(4,128)(2,1)S(1)}, bf16[16,4,256]{2,1,0:T(4,128)(2,1)}, u32[]{:S(2)}) copy-start(bf16[16,4,256]{2,1,0:T(4,128)(2,1)} %param.23) | copy-start | bytes 98308
  0.7 14.5 %copy-start.6 = (s32[16]{0:T(128)S(1)}, s32[16]{0:T(128)}, u32[]{:S(2)}) copy-start(s32[16]{0:T(128)} %param.25) | copy-start | bytes 196
  0.7 14.5 %copy-start.3 = (bf16[16,4,256]{2,1,0:T(4,128)(2,1)S(1)}, bf16[16,4,256]{2,1,0:T(4,128)(2,1)}, u32[]{:S(2)}) copy-start(bf16[16,4,256]{2,1,0:T(4,128)(2,1)} %param.24) | copy-start | bytes 98308
  3.3 20.7 %all-to-all-start = ((bf16[64,2,256]{2,1,0:T(2,128)(2,1)}), bf16[64,2,256]{2,1,0:T(2,128)(2,1)S(1)}, u32[]{:S(2)}, u32[]{:S(2)}) async-start(bf16[64,2,256]{2,1,0:T(2,128)(2,1)} %reshape.174), calls=%async_computation | async-start | bytes 131072 | tf_op jit(solution)/shard_map/all_to_all | solution.py:72
  22.3 35.1 %copy-start.1 = (f32[16,2,128,128]{3,2,1,0:T(8,128)}, f32[16,2,128,128]{3,2,1,0:T(8,128)S(1)}, u32[]{:S(2)}) copy-start(f32[16,2,128,128]{3,2,1,0:T(8,128)S(1)} %add_select_fusion) | copy-start | bytes 6291460
  22.3 7.6 %copy-start.7 = (f32[128]{0:T(128)S(1)}, f32[128]{0:T(128)}, u32[]{:S(2)}) copy-start(f32[128]{0:T(128)} %param.21) | copy-start | bytes 1540
  22.3 15.1 %copy-start.5 = (f32[2048]{0:T(1024)S(1)}, f32[2048]{0:T(1024)}, u32[]{:S(2)}) copy-start(f32[2048]{0:T(1024)} %param.14) | copy-start | bytes 24580
  25.4 11.4 %all-to-all-start.1 = ((bf16[4,4,4,2048]{3,1,2,0:T(4,128)(2,1)}), bf16[4,4,4,2048]{3,1,2,0:T(4,128)(2,1)S(1)}, u32[]{:S(2)}, u32[]{:S(2)}) async-start(bf16[4,4,4,2048]{3,1,2,0:T(4,128)(2,1)} %broadcast_in_dim.25), calls=%async_computation.1 | async-start | bytes 524288 | tf_op jit(solution)/shard_map/all_to_all | solution.py:15
where the time goes:
time: 116 us; the launch traced here: 115 us
  blocking collectives  42 us (36%)
  matrix products  28.8 us (25%)
  starting transfers between devices  16.1 us (14%)
  local copies, waits for them, and re-layouts  10.9 us (9%)
  waiting for transfers between devices  8.71 us (8%)
  other arithmetic  7.83 us (7%)
    all_to_all x2, blocking collectives, turned_blocks(): whole = lax.all_to_all(whole, axes[k], k, k, tiled=True)  20.8 us
    dot_general x4, matrix products, shards(): jnp.einsum('bhk,bhkv->bhv', query[:, step], state, precision=lax.Precisio...  20.3 us
    all_gather x1, blocking collectives, shards(): collected = lax.all_gather(stacked, 'tp', axis=1, tiled=True)  13.4 us
    all_to_all x1, starting transfers between devices, shards(): lax.all_to_all(source, KV, split_axis=0, concat_axis=2, tiled=True)  11.6 us
    all_to_all x1, blocking collectives, shards(): lax.all_to_all(mixed_heads, 'tp', split_axis=0, concat_axis=2, tiled=True)  7.8 us
    select_n x1, other arithmetic, shards(): state = jnp.where(live, moved, state)  7.02 us
    all_to_all x1, waiting for transfers between devices, copy_for_each(): return lax.all_to_all(copies, axis, split_axis=0, concat_axis=0, tiled=True)  6.94 us
    unnamed x24, local copies, waits for them, and re-layouts  4.47 us
  transfers between devices with their start and end apart: 2, of which 2 were waited for; matrix products, arithmetic and copies ran while one was open for 6% of the time, Pallas kernels for 0%

commit v1 on v0

v1 whole, which is shorter than its diff:
```python
import functools

import jax
import jax.numpy as jnp
from jax import lax
from jax.experimental import pallas as pl
from jax.experimental.pallas import tpu as pltpu
from jax.sharding import PartitionSpec as P

D = 2048
HD = 128
PROPS = 4
NKV = 64
NTP = 4
SEQ = 16
ROWS = SEQ * PROPS
F = D // NKV
MESH = pl.DeviceIdType.MESH
FAR_FIRST = (4, 3, 5, 2, 6, 1, 7, 0)
NEAR_FIRST = (0, 1, 7, 2, 6, 3, 5, 4)


def swap_blocks(parts):
    lane = lax.broadcasted_iota(jnp.int32, parts[0].shape, parts[0].ndim - 1)
    axis = parts[0].ndim - 1
    low = lane < 64
    even = (lane // 32) % 2 == 0
    a0, a1, a2, a3 = parts
    c0 = jnp.where(low, a0, pltpu.roll(a2, 64, axis))
    c2 = jnp.where(low, pltpu.roll(a0, 64, axis), a2)
    c1 = jnp.where(low, a1, pltpu.roll(a3, 64, axis))
    c3 = jnp.where(low, pltpu.roll(a1, 64, axis), a3)
    b0 = jnp.where(even, c0, pltpu.roll(c1, 32, axis))
    b1 = jnp.where(even, pltpu.roll(c0, 96, axis), c1)
    b2 = jnp.where(even, c2, pltpu.roll(c3, 32, axis))
    b3 = jnp.where(even, pltpu.roll(c2, 96, axis), c3)
    return b0, b1, b2, b3


def sigmoid(x):
    return jax.nn.sigmoid(x)


def kernel(
    x_hbm, gain_hbm, wq_hbm, wf_hbm, wi_hbm, wg_hbm, wo_hbm, floor_hbm, hgain_hbm,
    base_hbm, pf_hbm, pv_hbm, acc_hbm,
    mixed_ref, taken_ref,
    x_v, gain_v, w_v, wo_v, floor_v, hgain_v, base_v, pf_v, pv_v, acc_v,
    s0_v, tx1, rx1, pre_v, a_v, o_v, mh_v, tx2, rx2,
    lsem, ssem1, rsem1, ssem2, rsem2, ssem3, rsem3,
):
    kv = lax.axis_index("kv")
    tp = lax.axis_index("tp")
    z = kv // 8
    xc = kv % 8

    locals_ = [
        pltpu.make_async_copy(x_hbm, x_v, lsem.at[0]),
        pltpu.make_async_copy(pf_hbm, pf_v, lsem.at[1]),
        pltpu.make_async_copy(pv_hbm, pv_v, lsem.at[2]),
        pltpu.make_async_copy(acc_hbm, acc_v, lsem.at[3]),
        pltpu.make_async_copy(floor_hbm, floor_v, lsem.at[4]),
        pltpu.make_async_copy(base_hbm, base_v, lsem.at[5]),
        pltpu.make_async_copy(gain_hbm, gain_v, lsem.at[6]),
        pltpu.make_async_copy(wq_hbm, w_v.at[0], lsem.at[7]),
        pltpu.make_async_copy(wf_hbm, w_v.at[1], lsem.at[8]),
        pltpu.make_async_copy(wi_hbm, w_v.at[2], lsem.at[9]),
        pltpu.make_async_copy(wg_hbm, w_v.at[3], lsem.at[10]),
        pltpu.make_async_copy(hgain_hbm, hgain_v, lsem.at[11]),
        pltpu.make_async_copy(wo_hbm, wo_v, lsem.at[12]),
    ]
    for copy in locals_:
        copy.start()

    barrier = pltpu.get_barrier_semaphore()

    def greet(k, c):
        pl.semaphore_signal(barrier, inc=1, device_id={"kv": (kv + k) % NKV}, device_id_type=MESH)
        return c

    lax.fori_loop(1, NKV, greet, 0)
    for k in range(1, NTP):
        pl.semaphore_signal(barrier, inc=1, device_id={"tp": (tp + k) % NTP}, device_id_type=MESH)

    locals_[0].wait()
    for b in range(8):
        block = x_v[:, :, 128 * b : 128 * (b + 1)].reshape(128, 128)
        tx1[8 * b : 8 * (b + 1)] = jnp.transpose(block).reshape(8, SEQ, 128)

    pl.semaphore_wait(barrier, NKV - 1 + NTP - 1)

    def send1(zd, xd):
        d = zd * 8 + xd
        pltpu.make_async_remote_copy(
            src_ref=tx1.at[d], dst_ref=rx1.at[kv], send_sem=ssem1, recv_sem=rsem1.at[z],
            device_id={"kv": d}, device_id_type=MESH,
        ).start()

    for dist in FAR_FIRST:
        zd = (z + dist) % 8
        lax.fori_loop(1 if dist == 0 else 0, 8, lambda k, c: (send1(zd, (xc + k) % 8), c)[1], 0)
    rx1[kv] = tx1[kv]

    for i in range(1, 6):
        locals_[i].wait()
    fl = floor_v[...]
    row4 = lax.broadcasted_iota(jnp.int32, (PROPS, 2 * HD), 0)
    seq_lane = lax.broadcasted_iota(jnp.int32, (1, SEQ), 1)

    def state_step(s, c):
        count = jnp.sum(jnp.where(seq_lane == s, acc_v[...], 0), axis=1, keepdims=True)
        live = row4 < count
        f = fl + (1.0 - fl) * sigmoid(pf_v[s].astype(jnp.float32))
        k = jnp.where(live, 1.0 - f, 0.0)
        f = jnp.where(live, f, 1.0)
        v = pv_v[s].astype(jnp.float32)
        f0, f1, f2, f3 = (f[j : j + 1] for j in range(4))
        f23 = f2 * f3
        f123 = f1 * f23
        stack = jnp.concatenate(
            [f0 * f123, k[0:1] * f123, k[1:2] * f23, k[2:3] * f3, k[3:4], jnp.zeros((3, 2 * HD), jnp.float32)],
            axis=0,
        )
        for h in range(2):
            cols = jnp.transpose(stack[:, h * HD : (h + 1) * HD])
            new = cols[:, 0:1] * base_v[s, h]
            for j in range(4):
                new = new + cols[:, j + 1 : j + 2] * v[j : j + 1, h * HD : (h + 1) * HD]
            taken_ref[s, h] = new
            s0_v[s, h] = new.astype(jnp.bfloat16)
        return c

    lax.fori_loop(0, SEQ, state_step, 0)

    for i in range(6, 11):
        locals_[i].wait()
    squares = jnp.zeros((SEQ, 128), jnp.float32)
    for n, dist in enumerate(NEAR_FIRST):
        zs = (z + dist) % 8
        count = 7 if dist == 0 else 8
        group = rx1.at[pl.ds(0, count)] if dist == 0 else rx1.at[pl.ds(pl.multiple_of(zs * 8, 8), count)]
        pltpu.make_async_remote_copy(
            src_ref=group, dst_ref=group, send_sem=ssem1, recv_sem=rsem1.at[zs],
            device_id={"kv": kv}, device_id_type=MESH,
        ).wait_recv()
        vals = rx1[pl.ds(pl.multiple_of(zs * 8, 8), 8)].astype(jnp.float32)
        squares = squares + jnp.sum(vals * vals, axis=0)
        tiles = []
        for q in range(2):
            swapped = swap_blocks([vals[4 * q + i] for i in range(4)])
            gain = gain_v[:, pl.ds(pl.multiple_of(zs * 256 + q * 128, 128), 128)]
            tiles.append(jnp.concatenate([(part * gain).astype(jnp.bfloat16) for part in swapped], axis=0))
        lhs = jnp.concatenate(tiles, axis=1)
        for i in range(4):
            w = w_v[i, pl.ds(pl.multiple_of(zs * 256, 256), 256), :]
            prod = jnp.dot(lhs, w, preferred_element_type=jnp.float32)
            if n == 0:
                pre_v[i] = prod
            else:
                pre_v[i] += prod
    lane = lax.broadcasted_iota(jnp.int32, (SEQ, 128), 1)
    scale = jnp.concatenate(
        [
            lax.rsqrt(
                jnp.sum(jnp.where(lane // F == p, squares, 0.0), axis=1, keepdims=True) / D + 1e-06
            )
            for p in range(PROPS)
        ],
        axis=0,
    )

    def pre(i):
        return (pre_v[i] * scale).astype(jnp.bfloat16).astype(jnp.float32)

    q_all = pre(0)
    q_all = q_all * sigmoid(q_all)
    f_all = fl + (1.0 - fl) * sigmoid(pre(1))
    k_all = 1.0 - f_all
    v_all = pre(2)

    def at(arr, t):
        return arr[t * SEQ : (t + 1) * SEQ]

    decay = None
    for t in range(PROPS):
        decay = at(f_all, t) if t == 0 else decay * at(f_all, t)
        for h in range(2):
            a_v[h, t * SEQ : (t + 1) * SEQ, :] = (at(q_all, t) * decay)[:, h * HD : (h + 1) * HD]
    for s in range(SEQ):
        for h in range(2):
            lhs = a_v[h, pl.ds(s, PROPS, stride=SEQ), :].astype(jnp.bfloat16)
            o_v[h, pl.ds(s, PROPS, stride=SEQ), :] = jnp.dot(
                lhs, s0_v[s, h], preferred_element_type=jnp.float32
            )
    locals_[11].wait()
    hg = hgain_v[...]
    gate = pre(3)
    gate = gate * sigmoid(gate)
    for t in range(PROPS):
        weight = at(q_all, t)
        extra = [jnp.zeros((SEQ, HD), jnp.float32) for _ in range(2)]
        for j in range(t, -1, -1):
            term = weight * at(k_all, j)
            for h in range(2):
                c = jnp.sum(term[:, h * HD : (h + 1) * HD], axis=1, keepdims=True)
                extra[h] = extra[h] + c * at(v_all, j)[:, h * HD : (h + 1) * HD]
            weight = weight * at(f_all, j)
        for h in range(2):
            cols = slice(h * HD, (h + 1) * HD)
            o = o_v[h, t * SEQ : (t + 1) * SEQ, :] + extra[h]
            norm = lax.rsqrt(jnp.mean(o * o, axis=1, keepdims=True) + 1e-05)
            mh_v[tp, t * SEQ : (t + 1) * SEQ, cols] = (
                o * norm * hg * at(gate, t)[:, cols]
            ).astype(jnp.bfloat16)

    gathers = []
    for k in range(1, NTP):
        copy = pltpu.make_async_remote_copy(
            src_ref=mh_v.at[tp], dst_ref=mh_v.at[tp], send_sem=ssem2.at[k], recv_sem=rsem2.at[k],
            device_id={"tp": (tp + k) % NTP}, device_id_type=MESH,
        )
        copy.start()
        gathers.append(copy)
    locals_[12].wait()
    for copy in gathers:
        copy.wait()

    for dist in FAR_FIRST:
        zd = (z + dist) % 8
        out = None
        for a in range(NTP):
            w = wo_v[a * 256 : (a + 1) * 256, pl.ds(pl.multiple_of(zd * 256, 256), 256)]
            prod = jnp.dot(mh_v[a], w, preferred_element_type=jnp.float32)
            out = prod if out is None else out + prod
        for q in range(2):
            blocks = swap_blocks([out[p * SEQ : (p + 1) * SEQ, q * 128 : (q + 1) * 128] for p in range(PROPS)])
            for j in range(4):
                tx2[zd * 8 + 4 * q + j] = blocks[j].astype(jnp.bfloat16)

        def send2(k, c):
            d = zd * 8 + (xc + k) % 8
            pltpu.make_async_remote_copy(
                src_ref=tx2.at[d], dst_ref=rx2.at[kv], send_sem=ssem3, recv_sem=rsem3.at[z],
                device_id={"kv": d}, device_id_type=MESH,
            ).start()
            return c

        lax.fori_loop(1 if dist == 0 else 0, 8, send2, 0)
    rx2[kv] = tx2[kv]

    for dist in NEAR_FIRST:
        zs = (z + dist) % 8
        count = 7 if dist == 0 else 8
        group = rx2.at[pl.ds(0, count)] if dist == 0 else rx2.at[pl.ds(pl.multiple_of(zs * 8, 8), count)]
        pltpu.make_async_remote_copy(
            src_ref=group, dst_ref=group, send_sem=ssem3, recv_sem=rsem3.at[zs],
            device_id={"kv": kv}, device_id_type=MESH,
        ).wait_recv()
        block = rx2[pl.ds(pl.multiple_of(zs * 8, 8), 8)].reshape(128, 128)
        mixed_ref[:, :, pl.ds(pl.multiple_of(zs * 128, 128), 128)] = jnp.transpose(block).reshape(
            PROPS, F, 128
        )

    for tx, sem in ((tx1, ssem1), (tx2, ssem3)):
        sent = tx.at[pl.ds(0, NKV - 1)]
        pltpu.make_async_remote_copy(
            src_ref=sent, dst_ref=sent, send_sem=sem, recv_sem=sem,
            device_id={"kv": kv}, device_id_type=MESH,
        ).wait_send()


def shards(hidden, norm_gain, w_query, w_forget, w_input, w_outgate, w_out, floor, head_gain, base_state, prev_forget, prev_input, accepted):
    any_spec = pl.BlockSpec(memory_space=pl.ANY)
    vmem = pl.BlockSpec(memory_space=pltpu.VMEM)
    bf, f32 = jnp.bfloat16, jnp.float32
    mixed, taken = pl.pallas_call(
        kernel,
        name="verify",
        out_shape=(
            jax.ShapeDtypeStruct((PROPS, F, NKV * SEQ), bf),
            jax.ShapeDtypeStruct((SEQ, 2, HD, HD), f32),
        ),
        in_specs=[any_spec] * 13,
        out_specs=(vmem, vmem),
        scratch_shapes=[
            pltpu.VMEM((PROPS, F, NKV * SEQ), bf),
            pltpu.VMEM((1, D), f32),
            pltpu.VMEM((4, D, 256), bf),
            pltpu.VMEM((1024, D), bf),
            pltpu.VMEM((1, 256), f32),
            pltpu.VMEM((1, HD), f32),
            pltpu.VMEM((SEQ, 2, HD, HD), f32),
            pltpu.VMEM((SEQ, PROPS, 256), bf),
            pltpu.VMEM((SEQ, PROPS, 256), bf),
            pltpu.VMEM((1, SEQ), jnp.int32),
            pltpu.VMEM((SEQ, 2, HD, HD), bf),
            pltpu.VMEM((NKV, SEQ, 128), bf),
            pltpu.VMEM((NKV, SEQ, 128), bf),
            pltpu.VMEM((4, ROWS, 256), f32),
            pltpu.VMEM((2, ROWS, HD), f32),
            pltpu.VMEM((2, ROWS, HD), f32),
            pltpu.VMEM((NTP, ROWS, 256), bf),
            pltpu.VMEM((NKV, SEQ, 128), bf),
            pltpu.VMEM((NKV, SEQ, 128), bf),
            pltpu.SemaphoreType.DMA((13,)),
            pltpu.SemaphoreType.DMA,
            pltpu.SemaphoreType.DMA((8,)),
            pltpu.SemaphoreType.DMA((NTP,)),
            pltpu.SemaphoreType.DMA((NTP,)),
            pltpu.SemaphoreType.DMA,
            pltpu.SemaphoreType.DMA((8,)),
        ],
        compiler_params=pltpu.CompilerParams(collective_id=0, has_side_effects=True),
    )(
        jnp.transpose(hidden, (1, 2, 0)),
        norm_gain.reshape(1, -1),
        w_query, w_forget, w_input, w_outgate, w_out,
        floor.reshape(1, -1),
        head_gain.reshape(1, -1),
        base_state, prev_forget, prev_input,
        accepted.reshape(1, -1),
    )
    return jnp.transpose(mixed, (2, 0, 1)), taken


def solution(mesh):
    in_specs = (
        P(None, None, "kv"), P(), P(None, "tp"), P(None, "tp"), P(None, "tp"), P(None, "tp"), P(), P("tp"), P(),
        P("kv", "tp", None, None), P("kv", None, "tp"), P("kv", None, "tp"), P("kv"),
    )
    out_specs = (P(None, None, "kv"), P("kv", "tp", None, None))
    return jax.shard_map(shards, mesh=mesh, in_specs=in_specs, out_specs=out_specs, check_vma=False)
```

time: 116 us -> 45 us (0.39)
  the two profiles are of different devices: /device:TPU:32 before, /device:TPU:1 now
where the time goes in v1:
time: 45 us; the launch traced here: 44.8 us
  Pallas kernels  39.4 us (88%)
  local copies, waits for them, and re-layouts  4.8 us (11%)
  between operations  0.64 us (1%)
    pallas_call x1, Pallas kernels, shards(): pl.pallas_call(kernel, name='verify', out_shape=(jax.ShapeDtypeStruct((PR...  39.4 us
    unnamed x2, local copies, waits for them, and re-layouts  4.8 us

profile of v1, /device:TPU:1, one launch (start us, length us, event | category | flops | bytes accessed | tf_op | source)
XLA Modules:
  0.0 44.8 jit_solution(15587625558949626492)
XLA Ops:
  0.6 39.4 %verify.1 = (bf16[4,32,1024]{2,1,0:T(8,128)(2,1)}, f32[16,2,128,128]{3,2,1,0:T(8,128)}) custom-call(bf16[4,32,1024]{2,1,0:T(8,128)(2,1)} %bitcast.6, f32[1,2048]{1,0:T(1,128)} %bitcast.8, bf16[2048,256]{1,0:T(8,128)(2,1)} %wq_hbm.1, bf16[2048,256]{1,0:T(8,128)(2,1)} %wf_hbm.1, bf16[2048,256]{1,0:T(8,128)(2,1)} %wi_hbm.1, bf16[2048,256]{1,0:T(8,128)(2,1)} %wg_hbm.1, ...), custom_call_target="tpu_custom_call" | custom-call | tf_op jit(solution)/shard_map/verify/pallas_call | solution.py:276
  40.0 1.7 %copy.17 = bf16[1024,4,32]{0,2,1:T(8,128)(2,1)} copy(bf16[1024,4,32]{0,2,1:T(8,128)(2,1)} %bitcast.7) | data formatting | bytes 524288
  41.7 3.1 %copy.18 = f32[16,2,128,128]{3,2,1,0:T(8,128)} copy(f32[16,2,128,128]{3,2,1,0:T(8,128)} %get-tuple-element.9) | data formatting | bytes 4194304

commit v2 on v1

v2 whole, which is shorter than its diff:
```python
import functools

import jax
import jax.numpy as jnp
from jax import lax
from jax.experimental import pallas as pl
from jax.experimental.pallas import tpu as pltpu
from jax.sharding import PartitionSpec as P

D = 2048
HD = 128
PROPS = 4
NKV = 64
NTP = 4
SEQ = 16
ROWS = SEQ * PROPS
F = D // NKV
EARLY = 4
MESH = pl.DeviceIdType.MESH
FAR_FIRST = (3, 5, 2, 6, 1, 7, 0)


def swap_blocks(parts):
    lane = lax.broadcasted_iota(jnp.int32, parts[0].shape, parts[0].ndim - 1)
    axis = parts[0].ndim - 1
    low = lane < 64
    even = (lane // 32) % 2 == 0
    a0, a1, a2, a3 = parts
    c0 = jnp.where(low, a0, pltpu.roll(a2, 64, axis))
    c2 = jnp.where(low, pltpu.roll(a0, 64, axis), a2)
    c1 = jnp.where(low, a1, pltpu.roll(a3, 64, axis))
    c3 = jnp.where(low, pltpu.roll(a1, 64, axis), a3)
    b0 = jnp.where(even, c0, pltpu.roll(c1, 32, axis))
    b1 = jnp.where(even, pltpu.roll(c0, 96, axis), c1)
    b2 = jnp.where(even, c2, pltpu.roll(c3, 32, axis))
    b3 = jnp.where(even, pltpu.roll(c2, 96, axis), c3)
    return b0, b1, b2, b3


def sigmoid(x):
    return jax.nn.sigmoid(x)


def kernel(
    x_hbm, gain_hbm, wq_hbm, wf_hbm, wi_hbm, wg_hbm, wo_hbm, floor_hbm, hgain_hbm,
    base_hbm, pf_hbm, pv_hbm, acc_hbm,
    mixed_ref, taken_ref,
    x_v, gain_v, w_v, wo_v, floor_v, hgain_v, base_v, pf_v, pv_v, acc_v,
    s0_v, tx1, rx1, pre_v, a_v, o_v, mh_v, tx2, rx2,
    acc_o,
    lsem, ssem1, rsem1, ssem2, rsem2, ssem3, rsem3, rpair, fsem, rfwd,
):
    kv = lax.axis_index("kv")
    tp = lax.axis_index("tp")
    z = kv // 8
    xc = kv % 8
    z4 = (z + 4) % 8

    locals_ = [
        pltpu.make_async_copy(x_hbm, x_v, lsem.at[0]),
        pltpu.make_async_copy(pf_hbm, pf_v, lsem.at[1]),
        pltpu.make_async_copy(pv_hbm, pv_v, lsem.at[2]),
        pltpu.make_async_copy(acc_hbm, acc_v, lsem.at[3]),
        pltpu.make_async_copy(floor_hbm, floor_v, lsem.at[4]),
        pltpu.make_async_copy(base_hbm, base_v, lsem.at[5]),
        pltpu.make_async_copy(gain_hbm, gain_v, lsem.at[6]),
        pltpu.make_async_copy(wq_hbm, w_v.at[0], lsem.at[7]),
        pltpu.make_async_copy(wf_hbm, w_v.at[1], lsem.at[8]),
        pltpu.make_async_copy(wi_hbm, w_v.at[2], lsem.at[9]),
        pltpu.make_async_copy(wg_hbm, w_v.at[3], lsem.at[10]),
        pltpu.make_async_copy(hgain_hbm, hgain_v, lsem.at[11]),
        pltpu.make_async_copy(wo_hbm, wo_v, lsem.at[12]),
    ]
    for copy in locals_:
        copy.start()

    barrier = pltpu.get_barrier_semaphore()

    def greet(zd, xd):
        pl.semaphore_signal(barrier, inc=1, device_id={"kv": zd * 8 + xd}, device_id_type=MESH)

    for dist in (4,) + FAR_FIRST:
        for k in range(1 if dist == 0 else 0, 8):
            greet((z + dist) % 8, (xc + k) % 8)
    for k in range(1, NTP):
        pl.semaphore_signal(barrier, inc=1, device_id={"tp": (tp + k) % NTP}, device_id_type=MESH)

    locals_[0].wait()
    for b in range(8):
        block = x_v[:, :, 128 * b : 128 * (b + 1)].reshape(128, 128)
        tx1[8 * b : 8 * (b + 1)] = jnp.transpose(block).reshape(8, SEQ, 128)

    for i in range(1, 6):
        locals_[i].wait()
    fl = floor_v[...]
    row4 = lax.broadcasted_iota(jnp.int32, (PROPS, 2 * HD), 0)
    ones_row = (lax.broadcasted_iota(jnp.int32, (8, HD), 0) == 4).astype(jnp.float32)
    seq_lane = lax.broadcasted_iota(jnp.int32, (1, SEQ), 1)

    def state_step(s, c):
        count = jnp.sum(jnp.where(seq_lane == s, acc_v[...], 0), axis=1, keepdims=True)
        live = row4 < count
        f = fl + (1.0 - fl) * sigmoid(pf_v[s].astype(jnp.float32))
        k = jnp.where(live, 1.0 - f, 0.0)
        f = jnp.where(live, f, 1.0)
        v = pv_v[s].astype(jnp.float32)
        f0, f1, f2, f3 = (f[j : j + 1] for j in range(4))
        f23 = f2 * f3
        f123 = f1 * f23
        coef = jnp.concatenate(
            [k[0:1] * f123, k[1:2] * f23, k[2:3] * f3, k[3:4], f0 * f123, jnp.zeros((3, 2 * HD), jnp.float32)],
            axis=0,
        )
        high = coef.astype(jnp.bfloat16).astype(jnp.float32)
        rest = coef - high
        mid = rest.astype(jnp.bfloat16).astype(jnp.float32)
        lhs = jnp.concatenate([high, mid, rest - mid, jnp.zeros((8, 2 * HD), jnp.float32)], axis=0).astype(jnp.bfloat16)
        for h in range(2):
            cols = slice(h * HD, (h + 1) * HD)
            rows = jnp.concatenate([v[:, cols], jnp.zeros((4, HD), jnp.float32)], axis=0)
            rows = jnp.concatenate([ones_row, rows], axis=1)
            rhs = jnp.concatenate([rows] * 4, axis=0).astype(jnp.bfloat16)
            spread = lax.dot_general(
                lhs[:, cols], rhs, (((0,), (0,)), ((), ())), preferred_element_type=jnp.float32
            )
            new = spread[:, :HD] * base_v[s, h] + spread[:, HD:]
            taken_ref[s, h] = new
            s0_v[s, h] = new.astype(jnp.bfloat16)
        return c

    lax.fori_loop(0, EARLY, state_step, 0, unroll=4)

    pl.semaphore_wait(barrier, NKV - 1 + NTP - 1)

    def send_pair(tx, rx, send_sem, side):
        first = z4 * 8 + ((xc // 2 - tp + 4) % 4) * 2
        for k in range(2):
            pltpu.make_async_remote_copy(
                src_ref=tx.at[first + k], dst_ref=rx.at[kv], send_sem=send_sem, recv_sem=rpair.at[side],
                device_id={"kv": first + k}, device_id_type=MESH,
            ).start()

    def send_group(tx, rx, send_sem, recv_sem, dist):
        zd = (z + dist) % 8
        for k in range(1 if dist == 0 else 0, 8):
            d = zd * 8 + (xc + k) % 8
            pltpu.make_async_remote_copy(
                src_ref=tx.at[d], dst_ref=rx.at[kv], send_sem=send_sem, recv_sem=recv_sem.at[z],
                device_id={"kv": d}, device_id_type=MESH,
            ).start()

    def wait_group(rx, send_sem, recv_sem, dist):
        zs = (z + dist) % 8
        group = rx.at[pl.ds(0, 7)] if dist == 0 else rx.at[pl.ds(pl.multiple_of(zs * 8, 8), 8)]
        pltpu.make_async_remote_copy(
            src_ref=group, dst_ref=group, send_sem=send_sem, recv_sem=recv_sem.at[zs],
            device_id={"kv": kv}, device_id_type=MESH,
        ).wait_recv()

    def pass_on(rx, send_sem, side):
        pair = rx.at[pl.ds(z4 * 8 + ((xc // 2 + tp) % 4) * 2, 2)]
        pltpu.make_async_remote_copy(
            src_ref=pair, dst_ref=pair, send_sem=send_sem, recv_sem=rpair.at[side],
            device_id={"kv": kv}, device_id_type=MESH,
        ).wait_recv()
        copies = []
        for k in (2, 1, 3):
            copy = pltpu.make_async_remote_copy(
                src_ref=pair, dst_ref=pair, send_sem=fsem.at[side, k], recv_sem=rfwd.at[side, k],
                device_id={"tp": (tp + k) % NTP}, device_id_type=MESH,
            )
            copy.start()
            copies.append(copy)
        return copies

    def wait_far(rx, side):
        for k in (1, 3, 2):
            pair = rx.at[pl.ds(z4 * 8 + ((xc // 2 + tp - k + 4) % 4) * 2, 2)]
            pltpu.make_async_remote_copy(
                src_ref=pair, dst_ref=pair, send_sem=fsem.at[side, k], recv_sem=rfwd.at[side, k],
                device_id={"tp": (tp + k) % NTP}, device_id_type=MESH,
            ).wait_recv()

    send_pair(tx1, rx1, ssem1, 0)
    for dist in FAR_FIRST:
        send_group(tx1, rx1, ssem1, rsem1, dist)
    rx1[kv] = tx1[kv]

    lax.fori_loop(EARLY, SEQ, state_step, 0, unroll=4)
    passed = pass_on(rx1, ssem1, 0)
    for i in range(6, 11):
        locals_[i].wait()
    squares = jnp.zeros((SEQ, 128), jnp.float32)
    for n, dist in enumerate((0, 1, 7, 2, 6, 3, 5, 4)):
        zs = (z + dist) % 8
        if dist == 4:
            wait_far(rx1, 0)
        else:
            wait_group(rx1, ssem1, rsem1, dist)
        vals = rx1[pl.ds(pl.multiple_of(zs * 8, 8), 8)].astype(jnp.float32)
        squares = squares + jnp.sum(vals * vals, axis=0)
        tiles = []
        for q in range(2):
            swapped = swap_blocks([vals[4 * q + i] for i in range(4)])
            gain = gain_v[:, pl.ds(pl.multiple_of(zs * 256 + q * 128, 128), 128)]
            tiles.append(jnp.concatenate([(part * gain).astype(jnp.bfloat16) for part in swapped], axis=0))
        lhs = jnp.concatenate(tiles, axis=1)
        for i in range(4):
            w = w_v[i, pl.ds(pl.multiple_of(zs * 256, 256), 256), :]
            prod = jnp.dot(lhs, w, preferred_element_type=jnp.float32)
            if n == 0:
                pre_v[i] = prod
            else:
                pre_v[i] += prod
    lane = lax.broadcasted_iota(jnp.int32, (SEQ, 128), 1)
    scale = jnp.concatenate(
        [
            lax.rsqrt(
                jnp.sum(jnp.where(lane // F == p, squares, 0.0), axis=1, keepdims=True) / D + 1e-06
            )
            for p in range(PROPS)
        ],
        axis=0,
    )

    def pre(i):
        return (pre_v[i] * scale).astype(jnp.bfloat16).astype(jnp.float32)

    q_all = pre(0)
    q_all = q_all * sigmoid(q_all)
    f_all = fl + (1.0 - fl) * sigmoid(pre(1))
    k_all = 1.0 - f_all
    v_all = pre(2)

    def at(arr, t):
        return arr[t * SEQ : (t + 1) * SEQ]

    decay = None
    for t in range(PROPS):
        decay = at(f_all, t) if t == 0 else decay * at(f_all, t)
        for h in range(2):
            a_v[h, t * SEQ : (t + 1) * SEQ, :] = (at(q_all, t) * decay)[:, h * HD : (h + 1) * HD]
    locals_[11].wait()
    hg = hgain_v[...]
    gate = pre(3)
    gate = gate * sigmoid(gate)
    gathers = {}
    for h in range(2):
        cols = slice(h * HD, (h + 1) * HD)
        for s in range(SEQ):
            lhs = a_v[h, pl.ds(s, PROPS, stride=SEQ), :].astype(jnp.bfloat16)
            o_v[h, pl.ds(s, PROPS, stride=SEQ), :] = jnp.dot(lhs, s0_v[s, h], preferred_element_type=jnp.float32)
        for t in range(PROPS):
            weight = at(q_all, t)[:, cols]
            extra = jnp.zeros((SEQ, HD), jnp.float32)
            for j in range(t, -1, -1):
                c = jnp.sum(weight * at(k_all, j)[:, cols], axis=1, keepdims=True)
                extra = extra + c * at(v_all, j)[:, cols]
                if j:
                    weight = weight * at(f_all, j)[:, cols]
            o = o_v[h, t * SEQ : (t + 1) * SEQ, :] + extra
            norm = lax.rsqrt(jnp.mean(o * o, axis=1, keepdims=True) + 1e-05)
            mh_v[tp, h, t * SEQ : (t + 1) * SEQ, :] = (o * norm * hg * at(gate, t)[:, cols]).astype(jnp.bfloat16)
        for k in (2, 1, 3):
            gathers[k, h] = pltpu.make_async_remote_copy(
                src_ref=mh_v.at[tp, h], dst_ref=mh_v.at[tp, h], send_sem=ssem2.at[k, h], recv_sem=rsem2.at[k, h],
                device_id={"tp": (tp + k) % NTP}, device_id_type=MESH,
            )
            gathers[k, h].start()
    locals_[12].wait()

    def piece(k, cols):
        place = (tp - k + NTP) % NTP
        w = wo_v[pl.ds(pl.multiple_of(place * 256, 256), 256), cols]
        return jnp.dot(jnp.concatenate([mh_v[place, 0], mh_v[place, 1]], axis=1), w, preferred_element_type=jnp.float32)

    for k in (0, 1, 3):
        if k:
            gathers[k, 0].wait_recv()
            gathers[k, 1].wait_recv()
        for n in range(4):
            cols = slice(n * 512, (n + 1) * 512)
            if k:
                acc_o[:, cols] += piece(k, cols)
            else:
                acc_o[:, cols] = piece(k, cols)
    gathers[2, 0].wait_recv()
    gathers[2, 1].wait_recv()

    def finish(first, tiles):
        cols = pl.ds(pl.multiple_of(first * F, 128), tiles * 128)
        out = acc_o[:, cols] + piece(2, cols)
        for q in range(tiles):
            blocks = swap_blocks([out[p * SEQ : (p + 1) * SEQ, q * 128 : (q + 1) * 128] for p in range(PROPS)])
            for j in range(4):
                tx2[first + 4 * q + j] = blocks[j].astype(jnp.bfloat16)

    finish(z4 * 8 + ((xc // 2 - tp + 4) % 4) // 2 * 4, 1)
    send_pair(tx2, rx2, ssem3, 1)
    for dist in FAR_FIRST:
        finish((z + dist) % 8 * 8, 2)
        send_group(tx2, rx2, ssem3, rsem3, dist)
    rx2[kv] = tx2[kv]

    def place_group(dist):
        zs = (z + dist) % 8
        block = rx2[pl.ds(pl.multiple_of(zs * 8, 8), 8)].reshape(128, 128)
        mixed_ref[:, :, pl.ds(pl.multiple_of(zs * 128, 128), 128)] = jnp.transpose(block).reshape(
            PROPS, F, 128
        )

    passed += pass_on(rx2, ssem3, 1)
    for dist in (0, 1, 7, 2, 6, 3, 5):
        wait_group(rx2, ssem3, rsem3, dist)
        place_group(dist)
    wait_far(rx2, 1)
    place_group(4)
    for copy in passed:
        copy.wait_send()
    for copy in gathers.values():
        copy.wait_send()
    for tx, sem in ((tx1, ssem1), (tx2, ssem3)):
        sent = tx.at[pl.ds(0, NKV - 1 - 6)]
        pltpu.make_async_remote_copy(
            src_ref=sent, dst_ref=sent, send_sem=sem, recv_sem=sem,
            device_id={"kv": kv}, device_id_type=MESH,
        ).wait_send()


def tail(mixed_v, taken_v, mixed_hbm, taken_hbm, sem):
    copies = [pltpu.make_async_copy(mixed_v, mixed_hbm, sem.at[8])]
    for i in range(8):
        part = pl.ds(2 * i, 2)
        copies.append(pltpu.make_async_copy(taken_v.at[part], taken_hbm.at[part], sem.at[i]))
    for copy in copies:
        copy.start()
    for copy in copies:
        copy.wait()


def shards(hidden, norm_gain, w_query, w_forget, w_input, w_outgate, w_out, floor, head_gain, base_state, prev_forget, prev_input, accepted):
    any_spec = pl.BlockSpec(memory_space=pl.ANY)
    vmem = pl.BlockSpec(memory_space=pltpu.VMEM)
    bf, f32 = jnp.bfloat16, jnp.float32
    mixed, taken = pl.pallas_call(
        kernel,
        name="verify",
        out_shape=(
            pltpu.VMEM((PROPS, F, NKV * SEQ), bf),
            pltpu.VMEM((SEQ, 2, HD, HD), f32),
        ),
        in_specs=[any_spec] * 13,
        out_specs=(vmem, vmem),
        scratch_shapes=[
            pltpu.VMEM((PROPS, F, NKV * SEQ), bf),
            pltpu.VMEM((1, D), f32),
            pltpu.VMEM((4, D, 256), bf),
            pltpu.VMEM((1024, D), bf),
            pltpu.VMEM((1, 256), f32),
            pltpu.VMEM((1, HD), f32),
            pltpu.VMEM((SEQ, 2, HD, HD), f32),
            pltpu.VMEM((SEQ, PROPS, 256), bf),
            pltpu.VMEM((SEQ, PROPS, 256), bf),
            pltpu.VMEM((1, SEQ), jnp.int32),
            pltpu.VMEM((SEQ, 2, HD, HD), bf),
            pltpu.VMEM((NKV, SEQ, 128), bf),
            pltpu.VMEM((NKV, SEQ, 128), bf),
            pltpu.VMEM((4, ROWS, 256), f32),
            pltpu.VMEM((2, ROWS, HD), f32),
            pltpu.VMEM((2, ROWS, HD), f32),
            pltpu.VMEM((NTP, 2, ROWS, HD), bf),
            pltpu.VMEM((NKV, SEQ, 128), bf),
            pltpu.VMEM((NKV, SEQ, 128), bf),
            pltpu.VMEM((ROWS, D), f32),
            pltpu.SemaphoreType.DMA((13,)),
            pltpu.SemaphoreType.DMA,
            pltpu.SemaphoreType.DMA((8,)),
            pltpu.SemaphoreType.DMA((NTP, 2)),
            pltpu.SemaphoreType.DMA((NTP, 2)),
            pltpu.SemaphoreType.DMA,
            pltpu.SemaphoreType.DMA((8,)),
            pltpu.SemaphoreType.DMA((2,)),
            pltpu.SemaphoreType.DMA((2, NTP)),
            pltpu.SemaphoreType.DMA((2, NTP)),
        ],
        compiler_params=pltpu.CompilerParams(collective_id=0, has_side_effects=True),
    )(
        jnp.transpose(hidden, (1, 2, 0)),
        norm_gain.reshape(1, -1),
        w_query, w_forget, w_input, w_outgate, w_out,
        floor.reshape(1, -1),
        head_gain.reshape(1, -1),
        base_state, prev_forget, prev_input,
        accepted.reshape(1, -1),
    )
    mixed, taken = pl.pallas_call(
        tail,
        name="place",
        out_shape=(
            jax.ShapeDtypeStruct((PROPS, F, NKV * SEQ), bf),
            jax.ShapeDtypeStruct((SEQ, 2, HD, HD), f32),
        ),
        in_specs=[vmem] * 2,
        out_specs=(any_spec,) * 2,
        scratch_shapes=[pltpu.SemaphoreType.DMA((9,))],
    )(pltpu.with_memory_space_constraint(mixed, pltpu.VMEM), pltpu.with_memory_space_constraint(taken, pltpu.VMEM))
    return jnp.transpose(mixed, (2, 0, 1)), taken


def solution(mesh):
    in_specs = (
        P(None, None, "kv"), P(), P(None, "tp"), P(None, "tp"), P(None, "tp"), P(None, "tp"), P(), P("tp"), P(),
        P("kv", "tp", None, None), P("kv", None, "tp"), P("kv", None, "tp"), P("kv"),
    )
    out_specs = (P(None, None, "kv"), P("kv", "tp", None, None))
    return jax.shard_map(shards, mesh=mesh, in_specs=in_specs, out_specs=out_specs, check_vma=False)
```

time: 45 us -> 38.1 us (0.85)
  local copies, waits for them, and re-layouts: 4.8 us -> 0 us
  Pallas kernels: 39.4 us -> 37.4 us
    unnamed x2 -> x0, local copies, waits for them, and re-layouts: 4.8 us -> none
    pallas_call x1 -> x2, Pallas kernels: 39.4 us -> 37.4 us  [the longest x1 35.9 us: shards(): pl.pallas_call(kernel, name='verify', out_shape=(pltpu.VMEM((PROPS, F, NK...]
where the time goes in v2:
time: 38.1 us
  Pallas kernels  37.4 us (98%)
  between operations  0.64 us (2%)
    pallas_call x1, Pallas kernels, shards(): pl.pallas_call(kernel, name='verify', out_shape=(pltpu.VMEM((PROPS, F, NK...  35.9 us
    pallas_call x1, Pallas kernels, shards(): pl.pallas_call(tail, name='place', out_shape=(jax.ShapeDtypeStruct((PROPS...  1.47 us

profile of v2, /device:TPU:1, one launch (start us, length us, event | category | flops | bytes accessed | tf_op | source)
XLA Modules:
  0.0 38.1 jit_solution(2354224025620054978)
XLA Ops:
  0.6 35.9 %verify.1 = (bf16[4,32,1024]{2,1,0:T(8,128)(2,1)S(1)}, f32[16,2,128,128]{3,2,1,0:T(8,128)S(1)}) custom-call(bf16[4,32,1024]{2,1,0:T(8,128)(2,1)} %bitcast.6, f32[1,2048]{1,0:T(1,128)} %bitcast.7, bf16[2048,256]{1,0:T(8,128)(2,1)} %wq_hbm.1, bf16[2048,256]{1,0:T(8,128)(2,1)} %wf_hbm.1, bf16[2048,256]{1,0:T(8,128)(2,1)} %wi_hbm.1, bf16[2048,256]{1,0:T(8,128)(2,1)} %wg_hbm.1, ...), custom_call_target="tpu_custom_call" | custom-call | tf_op jit(solution)/shard_map/verify/pallas_call | solution.py:345
  36.6 1.5 %place.1 = (bf16[4,32,1024]{2,1,0:T(8,128)(2,1)}, f32[16,2,128,128]{3,2,1,0:T(8,128)}) custom-call(bf16[4,32,1024]{2,1,0:T(8,128)(2,1)S(1)} %get-tuple-element.6.mixed_v, f32[16,2,128,128]{3,2,1,0:T(8,128)S(1)} %get-tuple-element.7.taken_v), custom_call_target="tpu_custom_call" | custom-call | tf_op jit(solution)/shard_map/place/pallas_call | solution.py:396

commit v3 on v2

--- a/solution.py
+++ b/solution.py
@@ -17,7 +17,10 @@
 F = D // NKV
 EARLY = 4
 MESH = pl.DeviceIdType.MESH
-FAR_FIRST = (3, 5, 2, 6, 1, 7, 0)
+ORDER = (0, 1, 7, 2, 6, 3, 5, 4)
+RELAYED = (4, 3, 5)
+DIRECT = ((2, 6, 1, 7, 0), (3, 5, 2, 6, 1, 7, 0))
+HOLD = {3: 0, 5: 1, 4: 2}
 
 
 def swap_blocks(parts):
@@ -48,14 +51,19 @@
     x_v, gain_v, w_v, wo_v, floor_v, hgain_v, base_v, pf_v, pv_v, acc_v,
     s0_v, tx1, rx1, pre_v, a_v, o_v, mh_v, tx2, rx2,
     acc_o,
-    lsem, ssem1, rsem1, ssem2, rsem2, ssem3, rsem3, rpair, fsem, rfwd,
+    hold,
+    lsem, ssem, rsem, hsem, fsem, gsem, psem, qsem, ssem2, rsem2,
 ):
     kv = lax.axis_index("kv")
     tp = lax.axis_index("tp")
     z = kv // 8
     xc = kv % 8
-    z4 = (z + 4) % 8
-
+    mine = xc % 2
+    xr_base = xc // 2
+    turn = [(tp + 2 * mine + part) % 4 for part in range(2)]
+    xd = [(xr_base + 4 - turn[part]) % 4 for part in range(2)]
+
+    barrier = pltpu.get_barrier_semaphore()
     locals_ = [
         pltpu.make_async_copy(x_hbm, x_v, lsem.at[0]),
         pltpu.make_async_copy(pf_hbm, pf_v, lsem.at[1]),
@@ -71,19 +79,31 @@
         pltpu.make_async_copy(hgain_hbm, hgain_v, lsem.at[11]),
         pltpu.make_async_copy(wo_hbm, wo_v, lsem.at[12]),
     ]
-    for copy in locals_:
+    locals_[0].start()
+
+
+    def greet(where):
+        pl.semaphore_signal(barrier, inc=1, device_id=where, device_id_type=MESH)
+
+    for dist in RELAYED:
+        greet({"kv": (z + dist) % 8 * 8 + xc})
+    for part in range(2):
+        for r in (2, 1, 3, 0):
+            for m in range(2):
+                core = (mine + m) % 2
+                where = {"kv": z * 8 + (xr_base + r) % 4 * 2 + core, "tp": (r + 2 * core + 4 - part) % 4}
+                if r == 0 and m == 0:
+                    pl.when(turn[part] != 0)(functools.partial(greet, where))
+                else:
+                    greet(where)
+    for dist in DIRECT[0]:
+        for k in range(1 if dist == 0 else 0, 8):
+            greet({"kv": (z + dist) % 8 * 8 + (xc + 4 + k) % 8 if dist else z * 8 + (xc + k) % 8})
+    for k in range(1, NTP):
+        greet({"tp": (tp + k) % NTP})
+
+    for copy in locals_[1:]:
         copy.start()
-
-    barrier = pltpu.get_barrier_semaphore()
-
-    def greet(zd, xd):
-        pl.semaphore_signal(barrier, inc=1, device_id={"kv": zd * 8 + xd}, device_id_type=MESH)
-
-    for dist in (4,) + FAR_FIRST:
-        for k in range(1 if dist == 0 else 0, 8):
-            greet((z + dist) % 8, (xc + k) % 8)
-    for k in range(1, NTP):
-        pl.semaphore_signal(barrier, inc=1, device_id={"tp": (tp + k) % NTP}, device_id_type=MESH)
 
     locals_[0].wait()
     for b in range(8):
@@ -94,6 +114,7 @@
         locals_[i].wait()
     fl = floor_v[...]
     row4 = lax.broadcasted_iota(jnp.int32, (PROPS, 2 * HD), 0)
+    a_v[...] = jnp.zeros_like(a_v)
     ones_row = (lax.broadcasted_iota(jnp.int32, (8, HD), 0) == 4).astype(jnp.float32)
     seq_lane = lax.broadcasted_iota(jnp.int32, (1, SEQ), 1)
 
@@ -125,93 +146,132 @@
             )
             new = spread[:, :HD] * base_v[s, h] + spread[:, HD:]
             taken_ref[s, h] = new
-            s0_v[s, h] = new.astype(jnp.bfloat16)
+            s0_v[s, cols, :] = new.astype(jnp.bfloat16)
         return c
 
     lax.fori_loop(0, EARLY, state_step, 0, unroll=4)
 
-    pl.semaphore_wait(barrier, NKV - 1 + NTP - 1)
-
-    def send_pair(tx, rx, send_sem, side):
-        first = z4 * 8 + ((xc // 2 - tp + 4) % 4) * 2
+    others = (turn[0] + 3) // 4 + (turn[1] + 3) // 4
+    pl.semaphore_wait(barrier, 8 * len(DIRECT[0]) - 1 + len(RELAYED) + NTP - 1 + 14 + others)
+
+
+    def move(src, dst, send_sem, recv_sem, where):
+        return pltpu.make_async_remote_copy(
+            src_ref=src, dst_ref=dst, send_sem=send_sem, recv_sem=recv_sem, device_id=where, device_id_type=MESH
+        )
+
+    def send_relayed(dist):
+        zd = (z + dist) % 8
+        slot = HOLD[8 - dist]
+        move(
+            tx1.at[pl.ds(zd * 8 + xd[slot // 2] * 2, 2)], hold.at[slot], ssem.at[0], hsem.at[slot // 2],
+            {"kv": zd * 8 + xc},
+        ).start()
+
+    pair = (z + 4) % 8 * 8 + (xr_base + 4 - tp) % 4 * 2
+
+    def send_pair():
         for k in range(2):
-            pltpu.make_async_remote_copy(
-                src_ref=tx.at[first + k], dst_ref=rx.at[kv], send_sem=send_sem, recv_sem=rpair.at[side],
-                device_id={"kv": first + k}, device_id_type=MESH,
-            ).start()
-
-    def send_group(tx, rx, send_sem, recv_sem, dist):
+            move(tx2.at[pair + k], rx2.at[7, xc], ssem.at[1], psem, {"kv": pair + k}).start()
+
+    def send_direct(side, dist):
+        tx, rx = ((tx1, rx1), (tx2, rx2))[side]
         zd = (z + dist) % 8
+        slot = ORDER.index((8 - dist) % 8)
         for k in range(1 if dist == 0 else 0, 8):
             d = zd * 8 + (xc + k) % 8
-            pltpu.make_async_remote_copy(
-                src_ref=tx.at[d], dst_ref=rx.at[kv], send_sem=send_sem, recv_sem=recv_sem.at[z],
-                device_id={"kv": d}, device_id_type=MESH,
-            ).start()
-
-    def wait_group(rx, send_sem, recv_sem, dist):
-        zs = (z + dist) % 8
-        group = rx.at[pl.ds(0, 7)] if dist == 0 else rx.at[pl.ds(pl.multiple_of(zs * 8, 8), 8)]
-        pltpu.make_async_remote_copy(
-            src_ref=group, dst_ref=group, send_sem=send_sem, recv_sem=recv_sem.at[zs],
-            device_id={"kv": kv}, device_id_type=MESH,
-        ).wait_recv()
-
-    def pass_on(rx, send_sem, side):
-        pair = rx.at[pl.ds(z4 * 8 + ((xc // 2 + tp) % 4) * 2, 2)]
-        pltpu.make_async_remote_copy(
-            src_ref=pair, dst_ref=pair, send_sem=send_sem, recv_sem=rpair.at[side],
-            device_id={"kv": kv}, device_id_type=MESH,
-        ).wait_recv()
-        copies = []
-        for k in (2, 1, 3):
-            copy = pltpu.make_async_remote_copy(
-                src_ref=pair, dst_ref=pair, send_sem=fsem.at[side, k], recv_sem=rfwd.at[side, k],
-                device_id={"tp": (tp + k) % NTP}, device_id_type=MESH,
-            )
+            move(tx.at[d], rx.at[slot, xc], ssem.at[side], rsem.at[side, slot], {"kv": d}).start()
+
+    def pass_on(part):
+        held = hold.at[pl.ds(2 * part, 2 - part)]
+        to = rx1.at[pl.ds(5 + 2 * part, 2 - part)]
+        move(held, held, ssem.at[0], hsem.at[part], {"kv": kv}).wait_recv()
+        for m in range(2):
+            core = (mine + m) % 2
+            for k in (2, 1, 3, 0):
+                copy = move(
+                    held.at[:, core], to.at[:, xc], fsem.at[part], gsem.at[part],
+                    {"kv": z * 8 + xd[part] * 2 + core, "tp": (tp + k) % NTP},
+                )
+                if m == 0 and k == 0:
+                    pl.when(turn[part] != 0)(copy.start)
+
+                    @pl.when(turn[part] == 0)
+                    def _():
+                        for b in range(2 - part):
+                            rx1[5 + 2 * part + b, xc] = hold[2 * part + b, core]
+                else:
+                    copy.start()
+
+    def all_passed(part):
+        to = rx1.at[pl.ds(5 + 2 * part, 2 - part)]
+        less = rx1.at[pl.ds(5 + 2 * part, 2 - part), pl.ds(0, 7)]
+        return [move(ref, ref, fsem.at[part], gsem.at[part], {"kv": kv}) for ref in (to, less)]
+
+    def wait_passed(part):
+        full, less = all_passed(part)
+        pl.when(turn[part] != 0)(full.wait_recv)
+        pl.when(turn[part] == 0)(less.wait_recv)
+
+    def pair_at(k):
+        return rx2.at[7, pl.ds((xr_base + tp + k) % 4 * 2, 2)]
+
+    def pass_pair():
+        move(pair_at(0), pair_at(0), ssem.at[1], psem, {"kv": kv}).wait_recv()
+        copies = [
+            move(pair_at(0), pair_at(0), qsem.at[0, k], qsem.at[1, k], {"tp": (tp + k) % NTP}) for k in (2, 1, 3)
+        ]
+        for copy in copies:
             copy.start()
-            copies.append(copy)
         return copies
 
-    def wait_far(rx, side):
-        for k in (1, 3, 2):
-            pair = rx.at[pl.ds(z4 * 8 + ((xc // 2 + tp - k + 4) % 4) * 2, 2)]
-            pltpu.make_async_remote_copy(
-                src_ref=pair, dst_ref=pair, send_sem=fsem.at[side, k], recv_sem=rfwd.at[side, k],
-                device_id={"tp": (tp + k) % NTP}, device_id_type=MESH,
-            ).wait_recv()
-
-    send_pair(tx1, rx1, ssem1, 0)
-    for dist in FAR_FIRST:
-        send_group(tx1, rx1, ssem1, rsem1, dist)
-    rx1[kv] = tx1[kv]
+    def wait_direct(side, slot):
+        rx = (rx1, rx2)[side]
+        group = rx.at[slot, pl.ds(0, 7 if slot == 0 else 8)]
+        move(group, group, ssem.at[side], rsem.at[side, slot], {"kv": kv}).wait_recv()
+
+    for dist in RELAYED:
+        send_relayed(dist)
+    rx1[0, xc] = tx1[kv]
 
     lax.fori_loop(EARLY, SEQ, state_step, 0, unroll=4)
-    passed = pass_on(rx1, ssem1, 0)
+    for dist in DIRECT[0]:
+        send_direct(0, dist)
+    pass_on(0)
+    pass_on(1)
     for i in range(6, 11):
         locals_[i].wait()
     squares = jnp.zeros((SEQ, 128), jnp.float32)
-    for n, dist in enumerate((0, 1, 7, 2, 6, 3, 5, 4)):
-        zs = (z + dist) % 8
-        if dist == 4:
-            wait_far(rx1, 0)
-        else:
-            wait_group(rx1, ssem1, rsem1, dist)
-        vals = rx1[pl.ds(pl.multiple_of(zs * 8, 8), 8)].astype(jnp.float32)
-        squares = squares + jnp.sum(vals * vals, axis=0)
+
+    def take(n):
+        zs = (z + ORDER[n]) % 8
+        vals = rx1[n].astype(jnp.float32)
         tiles = []
         for q in range(2):
             swapped = swap_blocks([vals[4 * q + i] for i in range(4)])
             gain = gain_v[:, pl.ds(pl.multiple_of(zs * 256 + q * 128, 128), 128)]
             tiles.append(jnp.concatenate([(part * gain).astype(jnp.bfloat16) for part in swapped], axis=0))
         lhs = jnp.concatenate(tiles, axis=1)
+        prods = [
+            jnp.dot(lhs, w_v[i, pl.ds(pl.multiple_of(zs * 256, 256), 256), :], preferred_element_type=jnp.float32)
+            for i in range(4)
+        ]
+        return jnp.sum(vals * vals, axis=0), prods
+
+    for n in range(5):
+        wait_direct(0, n)
+        part, prods = take(n)
+        squares = squares + part
         for i in range(4):
-            w = w_v[i, pl.ds(pl.multiple_of(zs * 256, 256), 256), :]
-            prod = jnp.dot(lhs, w, preferred_element_type=jnp.float32)
             if n == 0:
-                pre_v[i] = prod
+                pre_v[i] = prods[i]
             else:
-                pre_v[i] += prod
+                pre_v[i] += prods[i]
+    wait_passed(0)
+    wait_passed(1)
+    last = [take(n) for n in (5, 6, 7)]
+    squares = squares + last[0][0] + last[1][0] + last[2][0]
+    sums = [pre_v[i] + (last[0][1][i] + last[1][1][i] + last[2][1][i]) for i in range(4)]
     lane = lax.broadcasted_iota(jnp.int32, (SEQ, 128), 1)
     scale = jnp.concatenate(
         [
@@ -224,7 +284,7 @@
     )
 
     def pre(i):
-        return (pre_v[i] * scale).astype(jnp.bfloat16).astype(jnp.float32)
+        return (sums[i] * scale).astype(jnp.bfloat16).astype(jnp.float32)
 
     q_all = pre(0)
     q_all = q_all * sigmoid(q_all)
@@ -238,8 +298,12 @@
     decay = None
     for t in range(PROPS):
         decay = at(f_all, t) if t == 0 else decay * at(f_all, t)
+        scaled = at(q_all, t) * decay
         for h in range(2):
-            a_v[h, t * SEQ : (t + 1) * SEQ, :] = (at(q_all, t) * decay)[:, h * HD : (h + 1) * HD]
+            a_v[h, pl.ds(4 * h + t, SEQ, stride=8), :] = scaled[:, h * HD : (h + 1) * HD]
+    for s in range(SEQ):
+        lhs = jnp.concatenate([a_v[0, 8 * s : 8 * s + 8], a_v[1, 8 * s : 8 * s + 8]], axis=1).astype(jnp.bfloat16)
+        o_v[8 * s : 8 * s + 8] = jnp.dot(lhs, s0_v[s], preferred_element_type=jnp.float32)
     locals_[11].wait()
     hg = hgain_v[...]
     gate = pre(3)
@@ -247,18 +311,13 @@
     gathers = {}
     for h in range(2):
         cols = slice(h * HD, (h + 1) * HD)
-        for s in range(SEQ):
-            lhs = a_v[h, pl.ds(s, PROPS, stride=SEQ), :].astype(jnp.bfloat16)
-            o_v[h, pl.ds(s, PROPS, stride=SEQ), :] = jnp.dot(lhs, s0_v[s, h], preferred_element_type=jnp.float32)
         for t in range(PROPS):
             weight = at(q_all, t)[:, cols]
-            extra = jnp.zeros((SEQ, HD), jnp.float32)
+            o = o_v[pl.ds(4 * h + t, SEQ, stride=8), :]
             for j in range(t, -1, -1):
-                c = jnp.sum(weight * at(k_all, j)[:, cols], axis=1, keepdims=True)
-                extra = extra + c * at(v_all, j)[:, cols]
+                o = o + jnp.sum(weight * at(k_all, j)[:, cols], axis=1, keepdims=True) * at(v_all, j)[:, cols]
                 if j:
                     weight = weight * at(f_all, j)[:, cols]
-            o = o_v[h, t * SEQ : (t + 1) * SEQ, :] + extra
             norm = lax.rsqrt(jnp.mean(o * o, axis=1, keepdims=True) + 1e-05)
             mh_v[tp, h, t * SEQ : (t + 1) * SEQ, :] = (o * norm * hg * at(gate, t)[:, cols]).astype(jnp.bfloat16)
         for k in (2, 1, 3):
@@ -287,44 +346,56 @@
     gathers[2, 0].wait_recv()
     gathers[2, 1].wait_recv()
 
-    def finish(first, tiles):
+    def product(first, tiles):
         cols = pl.ds(pl.multiple_of(first * F, 128), tiles * 128)
-        out = acc_o[:, cols] + piece(2, cols)
-        for q in range(tiles):
-            blocks = swap_blocks([out[p * SEQ : (p + 1) * SEQ, q * 128 : (q + 1) * 128] for p in range(PROPS)])
-            for j in range(4):
-                tx2[first + 4 * q + j] = blocks[j].astype(jnp.bfloat16)
-
-    finish(z4 * 8 + ((xc // 2 - tp + 4) % 4) // 2 * 4, 1)
-    send_pair(tx2, rx2, ssem3, 1)
-    for dist in FAR_FIRST:
-        finish((z + dist) % 8 * 8, 2)
-        send_group(tx2, rx2, ssem3, rsem3, dist)
-    rx2[kv] = tx2[kv]
-
-    def place_group(dist):
-        zs = (z + dist) % 8
-        block = rx2[pl.ds(pl.multiple_of(zs * 8, 8), 8)].reshape(128, 128)
-        mixed_ref[:, :, pl.ds(pl.multiple_of(zs * 128, 128), 128)] = jnp.transpose(block).reshape(
-            PROPS, F, 128
-        )
-
-    passed += pass_on(rx2, ssem3, 1)
-    for dist in (0, 1, 7, 2, 6, 3, 5):
-        wait_group(rx2, ssem3, rsem3, dist)
-        place_group(dist)
-    wait_far(rx2, 1)
-    place_group(4)
+        return acc_o[:, cols] + piece(2, cols)
+
+    def blocks_of(out):
+        found = []
+        for q in range(out.shape[1] // 128):
+            parts = [out[p * SEQ : (p + 1) * SEQ, q * 128 : (q + 1) * 128] for p in range(PROPS)]
+            found += [part.astype(jnp.bfloat16) for part in swap_blocks(parts)]
+        return found
+
+    chunks = [(pair // 4 * 4, 1)] + [((z + dist) % 8 * 8, 2) for dist in DIRECT[1]]
+    outs = [product(*chunks[0]), product(*chunks[1])]
+    ready = blocks_of(outs[0])
+    for n, (first, _) in enumerate(chunks):
+        if n + 2 < len(chunks):
+            outs.append(product(*chunks[n + 2]))
+        later = blocks_of(outs[n + 1]) if n + 1 < len(chunks) else None
+        for j, block in enumerate(ready):
+            tx2[first + j] = block
+        if n == 0:
+            send_pair()
+        else:
+            send_direct(1, DIRECT[1][n - 1])
+        ready = later
+    rx2[0, xc] = tx2[kv]
+    passed = pass_pair()
+
+    def place(n):
+        mixed_ref[:, :, pl.ds(pl.multiple_of((z + ORDER[n]) % 8 * 128, 128), 128)] = jnp.transpose(
+            rx2[n].reshape(128, 128)
+        ).reshape(PROPS, F, 128)
+
+    for n in (5, 6, 3, 4, 1, 2, 0):
+        wait_direct(1, n)
+        place(n)
+    for k in (1, 3, 2):
+        move(pair_at(4 - k), pair_at(4 - k), qsem.at[0, k], qsem.at[1, k], {"tp": tp}).wait_recv()
+    place(7)
+    for side, count in ((0, 8 * len(DIRECT[0]) - 1 + 6), (1, 8 * len(DIRECT[1]) - 1 + 2)):
+        sent = (tx1, tx2)[side].at[pl.ds(0, count)]
+        move(sent, sent, ssem.at[side], psem, {"kv": kv}).wait_send()
+    for part in range(2):
+        full, less = all_passed(part)
+        pl.when(turn[part] != 0)(full.wait_send)
+        pl.when(turn[part] == 0)(less.wait_send)
     for copy in passed:
         copy.wait_send()
     for copy in gathers.values():
         copy.wait_send()
-    for tx, sem in ((tx1, ssem1), (tx2, ssem3)):
-        sent = tx.at[pl.ds(0, NKV - 1 - 6)]
-        pltpu.make_async_remote_copy(
-            src_ref=sent, dst_ref=sent, send_sem=sem, recv_sem=sem,
-            device_id={"kv": kv}, device_id_type=MESH,
-        ).wait_send()
 
 
 def tail(mixed_v, taken_v, mixed_hbm, taken_hbm, sem):
@@ -362,26 +433,27 @@
             pltpu.VMEM((SEQ, PROPS, 256), bf),
             pltpu.VMEM((SEQ, PROPS, 256), bf),
             pltpu.VMEM((1, SEQ), jnp.int32),
-            pltpu.VMEM((SEQ, 2, HD, HD), bf),
+            pltpu.VMEM((SEQ, 2 * HD, HD), bf),
             pltpu.VMEM((NKV, SEQ, 128), bf),
-            pltpu.VMEM((NKV, SEQ, 128), bf),
+            pltpu.VMEM((8, 8, SEQ, 128), bf),
             pltpu.VMEM((4, ROWS, 256), f32),
-            pltpu.VMEM((2, ROWS, HD), f32),
-            pltpu.VMEM((2, ROWS, HD), f32),
+            pltpu.VMEM((2, 8 * SEQ, HD), f32),
+            pltpu.VMEM((8 * SEQ, HD), f32),
             pltpu.VMEM((NTP, 2, ROWS, HD), bf),
             pltpu.VMEM((NKV, SEQ, 128), bf),
-            pltpu.VMEM((NKV, SEQ, 128), bf),
+            pltpu.VMEM((8, 8, SEQ, 128), bf),
             pltpu.VMEM((ROWS, D), f32),
+            pltpu.VMEM((3, 2, SEQ, 128), bf),
             pltpu.SemaphoreType.DMA((13,)),
+            pltpu.SemaphoreType.DMA((2,)),
+            pltpu.SemaphoreType.DMA((2, 7)),
+            pltpu.SemaphoreType.DMA((2,)),
+            pltpu.SemaphoreType.DMA((2,)),
+            pltpu.SemaphoreType.DMA((2,)),
             pltpu.SemaphoreType.DMA,
-            pltpu.SemaphoreType.DMA((8,)),
+            pltpu.SemaphoreType.DMA((2, NTP)),
             pltpu.SemaphoreType.DMA((NTP, 2)),
             pltpu.SemaphoreType.DMA((NTP, 2)),
-            pltpu.SemaphoreType.DMA,
-            pltpu.SemaphoreType.DMA((8,)),
-            pltpu.SemaphoreType.DMA((2,)),
-            pltpu.SemaphoreType.DMA((2, NTP)),
-            pltpu.SemaphoreType.DMA((2, NTP)),
         ],
         compiler_params=pltpu.CompilerParams(collective_id=0, has_side_effects=True),
     )(

time: 38.1 us -> 37.4 us (0.982)
  Pallas kernels: 37.4 us -> 36.7 us
    pallas_call x1, Pallas kernels: 35.9 us -> 35.2 us  [shards(): pl.pallas_call(kernel, name='verify', out_shape=(pltpu.VMEM((PROPS, F, NK...]
where the time goes in v3:
time: 37.4 us; the launch traced here: 37.3 us
  Pallas kernels  36.7 us (98%)
  between operations  0.64 us (2%)
    pallas_call x1, Pallas kernels, shards(): pl.pallas_call(kernel, name='verify', out_shape=(pltpu.VMEM((PROPS, F, NK...  35.2 us
    pallas_call x1, Pallas kernels, shards(): pl.pallas_call(tail, name='place', out_shape=(jax.ShapeDtypeStruct((PROPS...  1.47 us

profile of v3, /device:TPU:1, one launch (start us, length us, event | category | flops | bytes accessed | tf_op | source)
XLA Modules:
  0.0 37.3 jit_solution(11018689580510376076)
XLA Ops:
  0.6 35.2 %verify.1 = (bf16[4,32,1024]{2,1,0:T(8,128)(2,1)S(1)}, f32[16,2,128,128]{3,2,1,0:T(8,128)S(1)}) custom-call(bf16[4,32,1024]{2,1,0:T(8,128)(2,1)} %bitcast.6, f32[1,2048]{1,0:T(1,128)} %bitcast.7, bf16[2048,256]{1,0:T(8,128)(2,1)} %wq_hbm.1, bf16[2048,256]{1,0:T(8,128)(2,1)} %wf_hbm.1, bf16[2048,256]{1,0:T(8,128)(2,1)} %wi_hbm.1, bf16[2048,256]{1,0:T(8,128)(2,1)} %wg_hbm.1, ...), custom_call_target="tpu_custom_call" | custom-call | tf_op jit(solution)/shard_map/verify/pallas_call | solution.py:416
  35.9 1.5 %place.1 = (bf16[4,32,1024]{2,1,0:T(8,128)(2,1)}, f32[16,2,128,128]{3,2,1,0:T(8,128)}) custom-call(bf16[4,32,1024]{2,1,0:T(8,128)(2,1)S(1)} %get-tuple-element.6.mixed_v, f32[16,2,128,128]{3,2,1,0:T(8,128)S(1)} %get-tuple-element.7.taken_v), custom_call_target="tpu_custom_call" | custom-call | tf_op jit(solution)/shard_map/place/pallas_call | solution.py:468

commit v4 on v3

--- a/solution.py
+++ b/solution.py
@@ -19,7 +19,8 @@
 MESH = pl.DeviceIdType.MESH
 ORDER = (0, 1, 7, 2, 6, 3, 5, 4)
 RELAYED = (4, 3, 5)
-DIRECT = ((2, 6, 1, 7, 0), (3, 5, 2, 6, 1, 7, 0))
+DIRECT = (2, 6, 1, 7, 0)
+UNITS = tuple(sorted(((zt, q) for zt in range(8) for q in range(2)), key=lambda u: (min(u[0], 4) + 1.2 * u[1], u)))
 HOLD = {3: 0, 5: 1, 4: 2}
 
 
@@ -48,11 +49,11 @@
     x_hbm, gain_hbm, wq_hbm, wf_hbm, wi_hbm, wg_hbm, wo_hbm, floor_hbm, hgain_hbm,
     base_hbm, pf_hbm, pv_hbm, acc_hbm,
     mixed_ref, taken_ref,
-    x_v, gain_v, w_v, wo_v, floor_v, hgain_v, base_v, pf_v, pv_v, acc_v,
+    x_v, small_v, w_v, wo_v, base_v, pfv_v, acc_v,
     s0_v, tx1, rx1, pre_v, a_v, o_v, mh_v, tx2, rx2,
     acc_o,
     hold,
-    lsem, ssem, rsem, hsem, fsem, gsem, psem, qsem, ssem2, rsem2,
+    lsem, ssem, rsem, hsem, fsem, gsem, osem, asem, bsem,
 ):
     kv = lax.axis_index("kv")
     tp = lax.axis_index("tp")
@@ -64,21 +65,25 @@
     xd = [(xr_base + 4 - turn[part]) % 4 for part in range(2)]
 
     barrier = pltpu.get_barrier_semaphore()
+    def local(src, dst, n):
+        return pltpu.make_async_copy(src, dst, lsem.at[n])
+
+    small = ((gain_hbm, 0, D), (floor_hbm, D, 256), (hgain_hbm, D + 256, HD))
     locals_ = [
-        pltpu.make_async_copy(x_hbm, x_v, lsem.at[0]),
-        pltpu.make_async_copy(pf_hbm, pf_v, lsem.at[1]),
-        pltpu.make_async_copy(pv_hbm, pv_v, lsem.at[2]),
-        pltpu.make_async_copy(acc_hbm, acc_v, lsem.at[3]),
-        pltpu.make_async_copy(floor_hbm, floor_v, lsem.at[4]),
-        pltpu.make_async_copy(base_hbm, base_v, lsem.at[5]),
-        pltpu.make_async_copy(gain_hbm, gain_v, lsem.at[6]),
-        pltpu.make_async_copy(wq_hbm, w_v.at[0], lsem.at[7]),
-        pltpu.make_async_copy(wf_hbm, w_v.at[1], lsem.at[8]),
-        pltpu.make_async_copy(wi_hbm, w_v.at[2], lsem.at[9]),
-        pltpu.make_async_copy(wg_hbm, w_v.at[3], lsem.at[10]),
-        pltpu.make_async_copy(hgain_hbm, hgain_v, lsem.at[11]),
-        pltpu.make_async_copy(wo_hbm, wo_v, lsem.at[12]),
+        local(x_hbm, x_v, 0),
+        local(pf_hbm, pfv_v.at[0], 1),
+        local(pv_hbm, pfv_v.at[1], 1),
+        local(acc_hbm, acc_v, 2),
+        *(local(ref, small_v.at[:, pl.ds(at, n)], 3) for ref, at, n in small),
+        local(base_hbm, base_v, 4),
+        *(local(ref, w_v.at[i], 5) for i, ref in enumerate((wq_hbm, wf_hbm, wi_hbm, wg_hbm))),
+        local(wo_hbm, wo_v, 6),
     ]
+    whole = [x_v, pfv_v, acc_v, small_v, base_v, w_v, wo_v]
+
+    def wait_local(n):
+        local(whole[n], whole[n], n).wait()
+
     locals_[0].start()
 
 
@@ -96,7 +101,7 @@
                     pl.when(turn[part] != 0)(functools.partial(greet, where))
                 else:
                     greet(where)
-    for dist in DIRECT[0]:
+    for dist in DIRECT:
         for k in range(1 if dist == 0 else 0, 8):
             greet({"kv": (z + dist) % 8 * 8 + (xc + 4 + k) % 8 if dist else z * 8 + (xc + k) % 8})
     for k in range(1, NTP):
@@ -105,14 +110,14 @@
     for copy in locals_[1:]:
         copy.start()
 
-    locals_[0].wait()
+    wait_local(0)
     for b in range(8):
         block = x_v[:, :, 128 * b : 128 * (b + 1)].reshape(128, 128)
         tx1[8 * b : 8 * (b + 1)] = jnp.transpose(block).reshape(8, SEQ, 128)
 
-    for i in range(1, 6):
-        locals_[i].wait()
-    fl = floor_v[...]
+    for n in range(1, 5):
+        wait_local(n)
+    fl = small_v[:, D : D + 256]
     row4 = lax.broadcasted_iota(jnp.int32, (PROPS, 2 * HD), 0)
     a_v[...] = jnp.zeros_like(a_v)
     ones_row = (lax.broadcasted_iota(jnp.int32, (8, HD), 0) == 4).astype(jnp.float32)
@@ -121,10 +126,10 @@
     def state_step(s, c):
         count = jnp.sum(jnp.where(seq_lane == s, acc_v[...], 0), axis=1, keepdims=True)
         live = row4 < count
-        f = fl + (1.0 - fl) * sigmoid(pf_v[s].astype(jnp.float32))
+        f = fl + (1.0 - fl) * sigmoid(pfv_v[0, s].astype(jnp.float32))
         k = jnp.where(live, 1.0 - f, 0.0)
         f = jnp.where(live, f, 1.0)
-        v = pv_v[s].astype(jnp.float32)
+        v = pfv_v[1, s].astype(jnp.float32)
         f0, f1, f2, f3 = (f[j : j + 1] for j in range(4))
         f23 = f2 * f3
         f123 = f1 * f23
@@ -152,7 +157,7 @@
     lax.fori_loop(0, EARLY, state_step, 0, unroll=4)
 
     others = (turn[0] + 3) // 4 + (turn[1] + 3) // 4
-    pl.semaphore_wait(barrier, 8 * len(DIRECT[0]) - 1 + len(RELAYED) + NTP - 1 + 14 + others)
+    pl.semaphore_wait(barrier, 8 * len(DIRECT) - 1 + len(RELAYED) + NTP - 1 + 14 + others)
 
 
     def move(src, dst, send_sem, recv_sem, where):
@@ -168,19 +173,16 @@
             {"kv": zd * 8 + xc},
         ).start()
 
-    pair = (z + 4) % 8 * 8 + (xr_base + 4 - tp) % 4 * 2
-
-    def send_pair():
-        for k in range(2):
-            move(tx2.at[pair + k], rx2.at[7, xc], ssem.at[1], psem, {"kv": pair + k}).start()
-
     def send_direct(side, dist):
         tx, rx = ((tx1, rx1), (tx2, rx2))[side]
         zd = (z + dist) % 8
         slot = ORDER.index((8 - dist) % 8)
         for k in range(1 if dist == 0 else 0, 8):
             d = zd * 8 + (xc + k) % 8
-            move(tx.at[d], rx.at[slot, xc], ssem.at[side], rsem.at[side, slot], {"kv": d}).start()
+            move(tx.at[d], rx.at[slot, xc], ssem.at[side], rsem.at[(slot + 1) // 2], {"kv": d}).start()
+
+    def other(k):
+        return tp if k == 3 else k + (k - tp + 4) // 4
 
     def pass_on(part):
         held = hold.at[pl.ds(2 * part, 2 - part)]
@@ -188,12 +190,12 @@
         move(held, held, ssem.at[0], hsem.at[part], {"kv": kv}).wait_recv()
         for m in range(2):
             core = (mine + m) % 2
-            for k in (2, 1, 3, 0):
+            for k in range(NTP):
                 copy = move(
-                    held.at[:, core], to.at[:, xc], fsem.at[part], gsem.at[part],
-                    {"kv": z * 8 + xd[part] * 2 + core, "tp": (tp + k) % NTP},
+                    held.at[:, core], to.at[:, xc], fsem, gsem,
+                    {"kv": z * 8 + xd[part] * 2 + core, "tp": other(k)},
                 )
-                if m == 0 and k == 0:
+                if m == 0 and k == 3:
                     pl.when(turn[part] != 0)(copy.start)
 
                     @pl.when(turn[part] == 0)
@@ -203,44 +205,25 @@
                 else:
                     copy.start()
 
-    def all_passed(part):
-        to = rx1.at[pl.ds(5 + 2 * part, 2 - part)]
-        less = rx1.at[pl.ds(5 + 2 * part, 2 - part), pl.ds(0, 7)]
-        return [move(ref, ref, fsem.at[part], gsem.at[part], {"kv": kv}) for ref in (to, less)]
-
-    def wait_passed(part):
-        full, less = all_passed(part)
-        pl.when(turn[part] != 0)(full.wait_recv)
-        pl.when(turn[part] == 0)(less.wait_recv)
-
-    def pair_at(k):
-        return rx2.at[7, pl.ds((xr_base + tp + k) % 4 * 2, 2)]
-
-    def pass_pair():
-        move(pair_at(0), pair_at(0), ssem.at[1], psem, {"kv": kv}).wait_recv()
-        copies = [
-            move(pair_at(0), pair_at(0), qsem.at[0, k], qsem.at[1, k], {"tp": (tp + k) % NTP}) for k in (2, 1, 3)
-        ]
-        for copy in copies:
-            copy.start()
-        return copies
-
-    def wait_direct(side, slot):
-        rx = (rx1, rx2)[side]
-        group = rx.at[slot, pl.ds(0, 7 if slot == 0 else 8)]
-        move(group, group, ssem.at[side], rsem.at[side, slot], {"kv": kv}).wait_recv()
+    def all_passed(wait):
+        for when, blocks in ((turn[0] == 0, 22), (turn[1] == 0, 23), (turn[0] * turn[1] != 0, 24)):
+            some = tx1.at[pl.ds(0, blocks)]
+            pl.when(when)(functools.partial(wait, move(some, some, fsem, gsem, {"kv": kv})))
+
+    def wait_direct(part):
+        group = rx1.at[pl.ds(1, 2)] if part else rx1.at[0, pl.ds(0, 7)]
+        move(group, group, ssem.at[0], rsem.at[part], {"kv": kv}).wait_recv()
 
     for dist in RELAYED:
         send_relayed(dist)
     rx1[0, xc] = tx1[kv]
 
     lax.fori_loop(EARLY, SEQ, state_step, 0, unroll=4)
-    for dist in DIRECT[0]:
+    for dist in DIRECT:
         send_direct(0, dist)
     pass_on(0)
     pass_on(1)
-    for i in range(6, 11):
-        locals_[i].wait()
+    wait_local(5)
     squares = jnp.zeros((SEQ, 128), jnp.float32)
 
     def take(n):
@@ -249,7 +232,7 @@
         tiles = []
         for q in range(2):
             swapped = swap_blocks([vals[4 * q + i] for i in range(4)])
-            gain = gain_v[:, pl.ds(pl.multiple_of(zs * 256 + q * 128, 128), 128)]
+            gain = small_v[:, pl.ds(pl.multiple_of(zs * 256 + q * 128, 128), 128)]
             tiles.append(jnp.concatenate([(part * gain).astype(jnp.bfloat16) for part in swapped], axis=0))
         lhs = jnp.concatenate(tiles, axis=1)
         prods = [
@@ -259,7 +242,8 @@
         return jnp.sum(vals * vals, axis=0), prods
 
     for n in range(5):
-        wait_direct(0, n)
+        if n in (0, 1, 3):
+            wait_direct((n + 1) // 2)
         part, prods = take(n)
         squares = squares + part
         for i in range(4):
@@ -267,8 +251,7 @@
                 pre_v[i] = prods[i]
             else:
                 pre_v[i] += prods[i]
-    wait_passed(0)
-    wait_passed(1)
+    all_passed(lambda copy: copy.wait_recv())
     last = [take(n) for n in (5, 6, 7)]
     squares = squares + last[0][0] + last[1][0] + last[2][0]
     sums = [pre_v[i] + (last[0][1][i] + last[1][1][i] + last[2][1][i]) for i in range(4)]
@@ -304,11 +287,9 @@
     for s in range(SEQ):
         lhs = jnp.concatenate([a_v[0, 8 * s : 8 * s + 8], a_v[1, 8 * s : 8 * s + 8]], axis=1).astype(jnp.bfloat16)
         o_v[8 * s : 8 * s + 8] = jnp.dot(lhs, s0_v[s], preferred_element_type=jnp.float32)
-    locals_[11].wait()
-    hg = hgain_v[...]
+    hg = small_v[:, D + 256 : D + 384]
     gate = pre(3)
     gate = gate * sigmoid(gate)
-    gathers = {}
     for h in range(2):
         cols = slice(h * HD, (h + 1) * HD)
         for t in range(PROPS):
@@ -320,13 +301,15 @@
                     weight = weight * at(f_all, j)[:, cols]
             norm = lax.rsqrt(jnp.mean(o * o, axis=1, keepdims=True) + 1e-05)
             mh_v[tp, h, t * SEQ : (t + 1) * SEQ, :] = (o * norm * hg * at(gate, t)[:, cols]).astype(jnp.bfloat16)
-        for k in (2, 1, 3):
-            gathers[k, h] = pltpu.make_async_remote_copy(
-                src_ref=mh_v.at[tp, h], dst_ref=mh_v.at[tp, h], send_sem=ssem2.at[k, h], recv_sem=rsem2.at[k, h],
-                device_id={"tp": (tp + k) % NTP}, device_id_type=MESH,
-            )
-            gathers[k, h].start()
-    locals_[12].wait()
+        for k in range(3):
+            there = mh_v.at[tp, h]
+            move(there, there, asem, bsem.at[(other(k) - tp + 3) % NTP], {"tp": other(k)}).start()
+
+    def wait_gather(k):
+        there = mh_v.at[(tp - k + NTP) % NTP]
+        move(there, there, asem, bsem.at[k - 1], {"tp": tp}).wait_recv()
+
+    wait_local(6)
 
     def piece(k, cols):
         place = (tp - k + NTP) % NTP
@@ -335,16 +318,14 @@
 
     for k in (0, 1, 3):
         if k:
-            gathers[k, 0].wait_recv()
-            gathers[k, 1].wait_recv()
+            wait_gather(k)
         for n in range(4):
             cols = slice(n * 512, (n + 1) * 512)
             if k:
                 acc_o[:, cols] += piece(k, cols)
             else:
                 acc_o[:, cols] = piece(k, cols)
-    gathers[2, 0].wait_recv()
-    gathers[2, 1].wait_recv()
+    wait_gather(2)
 
     def product(first, tiles):
         cols = pl.ds(pl.multiple_of(first * F, 128), tiles * 128)
@@ -357,7 +338,7 @@
             found += [part.astype(jnp.bfloat16) for part in swap_blocks(parts)]
         return found
 
-    chunks = [(pair // 4 * 4, 1)] + [((z + dist) % 8 * 8, 2) for dist in DIRECT[1]]
+    chunks = [(zt * 8 + 4 * q, 1) for zt, q in UNITS]
     outs = [product(*chunks[0]), product(*chunks[1])]
     ready = blocks_of(outs[0])
     for n, (first, _) in enumerate(chunks):
@@ -366,47 +347,41 @@
         later = blocks_of(outs[n + 1]) if n + 1 < len(chunks) else None
         for j, block in enumerate(ready):
             tx2[first + j] = block
-        if n == 0:
-            send_pair()
-        else:
-            send_direct(1, DIRECT[1][n - 1])
+        zt, q = UNITS[n]
+        slot = (z + 8 - zt) % 8
+        reach = (slot * (8 - slot) + 1) // 8
+        for k in range(4):
+            d = first + (xc + k) % 4
+            copy = move(tx2.at[d], rx2.at[slot, xc], ssem.at[1], osem.at[reach], {"kv": d})
+            if k:
+                copy.start()
+            else:
+                pl.when(d != kv)(copy.start)
         ready = later
     rx2[0, xc] = tx2[kv]
-    passed = pass_pair()
-
-    def place(n):
-        mixed_ref[:, :, pl.ds(pl.multiple_of((z + ORDER[n]) % 8 * 128, 128), 128)] = jnp.transpose(
-            rx2[n].reshape(128, 128)
+
+    for dist in ORDER:
+        if dist in (0, 1, 3):
+            group = (rx2.at[0, pl.ds(0, 7)], rx2.at[pl.ds(0, 4)], None, rx2.at[pl.ds(0, 3)])[dist]
+            move(group, group, ssem.at[1], osem.at[(dist + 1) // 2], {"kv": kv}).wait_recv()
+        mixed_ref[:, :, pl.ds(pl.multiple_of((z + dist) % 8 * 128, 128), 128)] = jnp.transpose(
+            rx2[dist].reshape(128, 128)
         ).reshape(PROPS, F, 128)
-
-    for n in (5, 6, 3, 4, 1, 2, 0):
-        wait_direct(1, n)
-        place(n)
-    for k in (1, 3, 2):
-        move(pair_at(4 - k), pair_at(4 - k), qsem.at[0, k], qsem.at[1, k], {"tp": tp}).wait_recv()
-    place(7)
-    for side, count in ((0, 8 * len(DIRECT[0]) - 1 + 6), (1, 8 * len(DIRECT[1]) - 1 + 2)):
+    for side, count in ((0, 8 * len(DIRECT) - 1 + 6), (1, NKV - 1)):
         sent = (tx1, tx2)[side].at[pl.ds(0, count)]
-        move(sent, sent, ssem.at[side], psem, {"kv": kv}).wait_send()
-    for part in range(2):
-        full, less = all_passed(part)
-        pl.when(turn[part] != 0)(full.wait_send)
-        pl.when(turn[part] == 0)(less.wait_send)
-    for copy in passed:
-        copy.wait_send()
-    for copy in gathers.values():
-        copy.wait_send()
+        move(sent, sent, ssem.at[side], hsem.at[0], {"kv": kv}).wait_send()
+    all_passed(lambda copy: copy.wait_send())
+    sent = mh_v.at[pl.ds(0, 3)]
+    move(sent, sent, asem, asem, {"tp": tp}).wait_send()
 
 
 def tail(mixed_v, taken_v, mixed_hbm, taken_hbm, sem):
-    copies = [pltpu.make_async_copy(mixed_v, mixed_hbm, sem.at[8])]
     for i in range(8):
         part = pl.ds(2 * i, 2)
-        copies.append(pltpu.make_async_copy(taken_v.at[part], taken_hbm.at[part], sem.at[i]))
-    for copy in copies:
-        copy.start()
-    for copy in copies:
-        copy.wait()
+        pltpu.make_async_copy(taken_v.at[part], taken_hbm.at[part], sem.at[0]).start()
+    pltpu.make_async_copy(mixed_v, mixed_hbm, sem.at[1]).start()
+    pltpu.make_async_copy(taken_v, taken_hbm, sem.at[0]).wait()
+    pltpu.make_async_copy(mixed_v, mixed_hbm, sem.at[1]).wait()
 
 
 def shards(hidden, norm_gain, w_query, w_forget, w_input, w_outgate, w_out, floor, head_gain, base_state, prev_forget, prev_input, accepted):
@@ -424,14 +399,11 @@
         out_specs=(vmem, vmem),
         scratch_shapes=[
             pltpu.VMEM((PROPS, F, NKV * SEQ), bf),
-            pltpu.VMEM((1, D), f32),
+            pltpu.VMEM((1, D + 384), f32),
             pltpu.VMEM((4, D, 256), bf),
             pltpu.VMEM((1024, D), bf),
-            pltpu.VMEM((1, 256), f32),
-            pltpu.VMEM((1, HD), f32),
             pltpu.VMEM((SEQ, 2, HD, HD), f32),
-            pltpu.VMEM((SEQ, PROPS, 256), bf),
-            pltpu.VMEM((SEQ, PROPS, 256), bf),
+            pltpu.VMEM((2, SEQ, PROPS, 256), bf),
             pltpu.VMEM((1, SEQ), jnp.int32),
             pltpu.VMEM((SEQ, 2 * HD, HD), bf),
             pltpu.VMEM((NKV, SEQ, 128), bf),
@@ -444,16 +416,15 @@
             pltpu.VMEM((8, 8, SEQ, 128), bf),
             pltpu.VMEM((ROWS, D), f32),
             pltpu.VMEM((3, 2, SEQ, 128), bf),
-            pltpu.SemaphoreType.DMA((13,)),
+            pltpu.SemaphoreType.DMA((7,)),
             pltpu.SemaphoreType.DMA((2,)),
-            pltpu.SemaphoreType.DMA((2, 7)),
-            pltpu.SemaphoreType.DMA((2,)),
-            pltpu.SemaphoreType.DMA((2,)),
+            pltpu.SemaphoreType.DMA((3,)),
             pltpu.SemaphoreType.DMA((2,)),
             pltpu.SemaphoreType.DMA,
-            pltpu.SemaphoreType.DMA((2, NTP)),
-            pltpu.SemaphoreType.DMA((NTP, 2)),
-            pltpu.SemaphoreType.DMA((NTP, 2)),
+            pltpu.SemaphoreType.DMA,
+            pltpu.SemaphoreType.DMA((3,)),
+            pltpu.SemaphoreType.DMA,
+            pltpu.SemaphoreType.DMA((3,)),
         ],
         compiler_params=pltpu.CompilerParams(collective_id=0, has_side_effects=True),
     )(
@@ -474,7 +445,7 @@
         ),
         in_specs=[vmem] * 2,
         out_specs=(any_spec,) * 2,
-        scratch_shapes=[pltpu.SemaphoreType.DMA((9,))],
+        scratch_shapes=[pltpu.SemaphoreType.DMA((2,))],
     )(pltpu.with_memory_space_constraint(mixed, pltpu.VMEM), pltpu.with_memory_space_constraint(taken, pltpu.VMEM))
     return jnp.transpose(mixed, (2, 0, 1)), taken
 

time: 37.4 us -> 34.7 us (0.928)
  Pallas kernels: 36.7 us -> 33.9 us
    pallas_call x1, Pallas kernels: 35.2 us -> 32.5 us  [shards(): pl.pallas_call(kernel, name='verify', out_shape=(pltpu.VMEM((PROPS, F, NK...]
where the time goes in v4:
time: 34.7 us; the launch traced here: 34.6 us
  Pallas kernels  33.9 us (98%)
  between operations  0.64 us (2%)
    pallas_call x1, Pallas kernels, shards(): pl.pallas_call(kernel, name='verify', out_shape=(pltpu.VMEM((PROPS, F, NK...  32.5 us
    pallas_call x1, Pallas kernels, shards(): pl.pallas_call(tail, name='place', out_shape=(jax.ShapeDtypeStruct((PROPS...  1.41 us

profile of v4, /device:TPU:1, one launch (start us, length us, event | category | flops | bytes accessed | tf_op | source)
XLA Modules:
  0.0 34.6 jit_solution(2573652407046502622)
XLA Ops:
  0.6 32.5 %verify.1 = (bf16[4,32,1024]{2,1,0:T(8,128)(2,1)S(1)}, f32[16,2,128,128]{3,2,1,0:T(8,128)S(1)}) custom-call(bf16[4,32,1024]{2,1,0:T(8,128)(2,1)} %bitcast.6, f32[1,2048]{1,0:T(1,128)} %bitcast.7, bf16[2048,256]{1,0:T(8,128)(2,1)} %wq_hbm.1, bf16[2048,256]{1,0:T(8,128)(2,1)} %wf_hbm.1, bf16[2048,256]{1,0:T(8,128)(2,1)} %wi_hbm.1, bf16[2048,256]{1,0:T(8,128)(2,1)} %wg_hbm.1, ...), custom_call_target="tpu_custom_call" | custom-call | tf_op jit(solution)/shard_map/verify/pallas_call | solution.py:391
  33.1 1.4 %place.1 = (bf16[4,32,1024]{2,1,0:T(8,128)(2,1)}, f32[16,2,128,128]{3,2,1,0:T(8,128)}) custom-call(bf16[4,32,1024]{2,1,0:T(8,128)(2,1)S(1)} %get-tuple-element.6.mixed_v, f32[16,2,128,128]{3,2,1,0:T(8,128)S(1)} %get-tuple-element.7.taken_v), custom_call_target="tpu_custom_call" | custom-call | tf_op jit(solution)/shard_map/place/pallas_call | solution.py:439

commit v5 on v4

--- a/solution.py
+++ b/solution.py
@@ -27,18 +27,14 @@
 def swap_blocks(parts):
     lane = lax.broadcasted_iota(jnp.int32, parts[0].shape, parts[0].ndim - 1)
     axis = parts[0].ndim - 1
-    low = lane < 64
-    even = (lane // 32) % 2 == 0
-    a0, a1, a2, a3 = parts
-    c0 = jnp.where(low, a0, pltpu.roll(a2, 64, axis))
-    c2 = jnp.where(low, pltpu.roll(a0, 64, axis), a2)
-    c1 = jnp.where(low, a1, pltpu.roll(a3, 64, axis))
-    c3 = jnp.where(low, pltpu.roll(a1, 64, axis), a3)
-    b0 = jnp.where(even, c0, pltpu.roll(c1, 32, axis))
-    b1 = jnp.where(even, pltpu.roll(c0, 96, axis), c1)
-    b2 = jnp.where(even, c2, pltpu.roll(c3, 32, axis))
-    b3 = jnp.where(even, pltpu.roll(c2, 96, axis), c3)
-    return b0, b1, b2, b3
+    place = lane // 32
+    found = []
+    for i in range(4):
+        block = parts[i]
+        for r in range(1, 4):
+            block = jnp.where(place == (i + r) % 4, pltpu.roll(parts[(i + r) % 4], 32 * r, axis), block)
+        found.append(block)
+    return found
 
 
 def sigmoid(x):

time: 34.7 us -> 34.6 us (level)
  no operation moved by 1% of the time
where the time goes in v5:
time: 34.6 us; the launch traced here: 34.5 us
  Pallas kernels  33.9 us (98%)
  between operations  0.64 us (2%)
    pallas_call x1, Pallas kernels, shards(): pl.pallas_call(kernel, name='verify', out_shape=(pltpu.VMEM((PROPS, F, NK...  32.5 us
    pallas_call x1, Pallas kernels, shards(): pl.pallas_call(tail, name='place', out_shape=(jax.ShapeDtypeStruct((PROPS...  1.41 us

profile of v5, /device:TPU:1, one launch (start us, length us, event | category | flops | bytes accessed | tf_op | source)
XLA Modules:
  0.0 34.5 jit_solution(12941644729016020625)
XLA Ops:
  0.6 32.5 %verify.1 = (bf16[4,32,1024]{2,1,0:T(8,128)(2,1)S(1)}, f32[16,2,128,128]{3,2,1,0:T(8,128)S(1)}) custom-call(bf16[4,32,1024]{2,1,0:T(8,128)(2,1)} %bitcast.6, f32[1,2048]{1,0:T(1,128)} %bitcast.7, bf16[2048,256]{1,0:T(8,128)(2,1)} %wq_hbm.1, bf16[2048,256]{1,0:T(8,128)(2,1)} %wf_hbm.1, bf16[2048,256]{1,0:T(8,128)(2,1)} %wi_hbm.1, bf16[2048,256]{1,0:T(8,128)(2,1)} %wg_hbm.1, ...), custom_call_target="tpu_custom_call" | custom-call | tf_op jit(solution)/shard_map/verify/pallas_call | solution.py:387
  33.1 1.4 %place.1 = (bf16[4,32,1024]{2,1,0:T(8,128)(2,1)}, f32[16,2,128,128]{3,2,1,0:T(8,128)}) custom-call(bf16[4,32,1024]{2,1,0:T(8,128)(2,1)S(1)} %get-tuple-element.6.mixed_v, f32[16,2,128,128]{3,2,1,0:T(8,128)S(1)} %get-tuple-element.7.taken_v), custom_call_target="tpu_custom_call" | custom-call | tf_op jit(solution)/shard_map/place/pallas_call | solution.py:435

commit v6 on v5

--- a/solution.py
+++ b/solution.py
@@ -57,7 +57,7 @@
     xc = kv % 8
     mine = xc % 2
     xr_base = xc // 2
-    turn = [(tp + 2 * mine + part) % 4 for part in range(2)]
+    turn = [(1 * tp + 2 * mine + 2 * part + 1) % 4 for part in range(2)]
     xd = [(xr_base + 4 - turn[part]) % 4 for part in range(2)]
 
     barrier = pltpu.get_barrier_semaphore()
@@ -92,7 +92,7 @@
         for r in (2, 1, 3, 0):
             for m in range(2):
                 core = (mine + m) % 2
-                where = {"kv": z * 8 + (xr_base + r) % 4 * 2 + core, "tp": (r + 2 * core + 4 - part) % 4}
+                where = {"kv": z * 8 + (xr_base + r) % 4 * 2 + core, "tp": 1 * (r + 2 * core + 2 * part + 3) % 4}
                 if r == 0 and m == 0:
                     pl.when(turn[part] != 0)(functools.partial(greet, where))
                 else:

time: 34.6 us -> 34.1 us (0.986)
  Pallas kernels: 33.9 us -> 33.3 us
    pallas_call x1, Pallas kernels: 32.5 us -> 31.9 us  [shards(): pl.pallas_call(kernel, name='verify', out_shape=(pltpu.VMEM((PROPS, F, NK...]
where the time goes in v6:
time: 34.1 us; the launch traced here: 34 us
  Pallas kernels  33.3 us (98%)
  between operations  0.64 us (2%)
    pallas_call x1, Pallas kernels, shards(): pl.pallas_call(kernel, name='verify', out_shape=(pltpu.VMEM((PROPS, F, NK...  31.9 us
    pallas_call x1, Pallas kernels, shards(): pl.pallas_call(tail, name='place', out_shape=(jax.ShapeDtypeStruct((PROPS...  1.41 us

profile of v6, /device:TPU:1, one launch (start us, length us, event | category | flops | bytes accessed | tf_op | source)
XLA Modules:
  0.0 34.0 jit_solution(10217794589317113009)
XLA Ops:
  0.6 31.9 %verify.1 = (bf16[4,32,1024]{2,1,0:T(8,128)(2,1)S(1)}, f32[16,2,128,128]{3,2,1,0:T(8,128)S(1)}) custom-call(bf16[4,32,1024]{2,1,0:T(8,128)(2,1)} %bitcast.6, f32[1,2048]{1,0:T(1,128)} %bitcast.7, bf16[2048,256]{1,0:T(8,128)(2,1)} %wq_hbm.1, bf16[2048,256]{1,0:T(8,128)(2,1)} %wf_hbm.1, bf16[2048,256]{1,0:T(8,128)(2,1)} %wi_hbm.1, bf16[2048,256]{1,0:T(8,128)(2,1)} %wg_hbm.1, ...), custom_call_target="tpu_custom_call" | custom-call | tf_op jit(solution)/shard_map/verify/pallas_call | solution.py:387
  32.6 1.4 %place.1 = (bf16[4,32,1024]{2,1,0:T(8,128)(2,1)}, f32[16,2,128,128]{3,2,1,0:T(8,128)}) custom-call(bf16[4,32,1024]{2,1,0:T(8,128)(2,1)S(1)} %get-tuple-element.6.mixed_v, f32[16,2,128,128]{3,2,1,0:T(8,128)S(1)} %get-tuple-element.7.taken_v), custom_call_target="tpu_custom_call" | custom-call | tf_op jit(solution)/shard_map/place/pallas_call | solution.py:435

commit v7 on v6

--- a/solution.py
+++ b/solution.py
@@ -15,7 +15,7 @@
 SEQ = 16
 ROWS = SEQ * PROPS
 F = D // NKV
-EARLY = 4
+EARLY = 8
 MESH = pl.DeviceIdType.MESH
 ORDER = (0, 1, 7, 2, 6, 3, 5, 4)
 RELAYED = (4, 3, 5)

time: 34.1 us -> 34.1 us (level)
  no operation moved by 1% of the time
where the time goes in v7:
time: 34.1 us; the launch traced here: 34 us
  Pallas kernels  33.3 us (98%)
  between operations  0.64 us (2%)
    pallas_call x1, Pallas kernels, shards(): pl.pallas_call(kernel, name='verify', out_shape=(pltpu.VMEM((PROPS, F, NK...  31.9 us
    pallas_call x1, Pallas kernels, shards(): pl.pallas_call(tail, name='place', out_shape=(jax.ShapeDtypeStruct((PROPS...  1.41 us

profile of v7, /device:TPU:1, one launch (start us, length us, event | category | flops | bytes accessed | tf_op | source)
XLA Modules:
  0.0 34.0 jit_solution(9569271690063507617)
XLA Ops:
  0.6 31.9 %verify.1 = (bf16[4,32,1024]{2,1,0:T(8,128)(2,1)S(1)}, f32[16,2,128,128]{3,2,1,0:T(8,128)S(1)}) custom-call(bf16[4,32,1024]{2,1,0:T(8,128)(2,1)} %bitcast.6, f32[1,2048]{1,0:T(1,128)} %bitcast.7, bf16[2048,256]{1,0:T(8,128)(2,1)} %wq_hbm.1, bf16[2048,256]{1,0:T(8,128)(2,1)} %wf_hbm.1, bf16[2048,256]{1,0:T(8,128)(2,1)} %wi_hbm.1, bf16[2048,256]{1,0:T(8,128)(2,1)} %wg_hbm.1, ...), custom_call_target="tpu_custom_call" | custom-call | tf_op jit(solution)/shard_map/verify/pallas_call | solution.py:387
  32.6 1.4 %place.1 = (bf16[4,32,1024]{2,1,0:T(8,128)(2,1)}, f32[16,2,128,128]{3,2,1,0:T(8,128)}) custom-call(bf16[4,32,1024]{2,1,0:T(8,128)(2,1)S(1)} %get-tuple-element.6.mixed_v, f32[16,2,128,128]{3,2,1,0:T(8,128)S(1)} %get-tuple-element.7.taken_v), custom_call_target="tpu_custom_call" | custom-call | tf_op jit(solution)/shard_map/place/pallas_call | solution.py:435
